TPU v7x, 32 devices: a whole 2x2x4 slice. The times are simulated.
32 devices in a mesh: sp: 8 (over z, x), tp: 4 (over y, core).
Axes of the slice: x: 2, y: 2, z: 4, core: 2. Of those that a mesh axis runs over, the one named last changes fastest.
Arguments:
- latents: bfloat16 [4096, 2048], P(('sp', 'tp')), may hold values from -6 to 6
- context: bfloat16 [512, 2048], P('sp'), may hold values from -6 to 6
- cond: float32 [2048], P('sp'), may hold values from -6 to 6
- ctx_cond: float32 [2048], P('sp'), may hold values from -6 to 6
- mod_weight: float32 [2048, 6144], P('sp', 'tp'), may hold values from -0.125 to 0.125
- query_weight: bfloat16 [2048, 2048], P(None, 'tp'), may hold values from -1 to 1, as said below
- key_matrix: bfloat16 [2048, 1024], P(None, 'tp'), may hold values from -1 to 1, as said below
- value_matrix: bfloat16 [2048, 1024], P(None, 'tp'), may hold values from -0.125 to 0.125
- out_weight: bfloat16 [2048, 2048], P('tp'), may hold values from -0.125 to 0.125
- query_gain: float32 [128], replicated, may hold values from 0.7 to 7
- key_gain: float32 [128], replicated, may hold values from 0.7 to 7
Outputs:
- updated: bfloat16 [4096, 2048], P(('sp', 'tp'))
Inputs may be any that keep to these rules, and one draw needn't show every extreme that they name: `query_weight`: entries of order 2048 to the power -1/2. `key_matrix`: entries of order 2048 to the power -1/2.
All inputs are finite; a program needn't handle non-finite values.
Results may differ from a plain program's by a relative error of at most 0.0085.
The roundings to bfloat16 on the way count: a program that leaves them out, or rounds other values in their place, can miss the bound.
Values may be sent and summed in bfloat16 or wider, within the bound.
A program may use at most 128 MiB of HBM per device.

v0:
```python
import math

import jax
import jax.numpy as jnp
from jax import lax
from jax.sharding import PartitionSpec as P

GRID_W = 64


NORM_EPS = 1e-06
ROPE_BASE = 10000.0


def normalize(latent_value_rows):
    return latent_value_rows * lax.rsqrt(
        jnp.mean(latent_value_rows * latent_value_rows, axis=-1, keepdims=True) + NORM_EPS
    )


def rotate(latent_value_rows, positions):
    quarter = latent_value_rows.shape[-1] // 2
    inv_freq = ROPE_BASE ** (-jnp.arange(quarter, dtype=jnp.float32) / quarter)
    angles = positions.astype(jnp.float32)[:, None] * inv_freq[None, :]
    cos_table = jnp.cos(angles)[:, None, :]
    sin_table = jnp.sin(angles)[:, None, :]
    first, second = (latent_value_rows[..., :quarter], latent_value_rows[..., quarter:])
    return jnp.concatenate(
        [first * cos_table - second * sin_table, second * cos_table + first * sin_table], axis=-1
    )


def axial(latent_value_rows, positions):
    half_dim = latent_value_rows.shape[-1] // 2
    return jnp.concatenate(
        [
            rotate(latent_value_rows[..., :half_dim], positions // GRID_W),
            rotate(latent_value_rows[..., half_dim:], positions % GRID_W),
        ],
        axis=-1,
    )


def modulate(latent_value_rows, mod_row):
    model_width = latent_value_rows.shape[-1]
    shift_vec = mod_row[:model_width]
    scale_vec = mod_row[model_width : 2 * model_width]
    return (
        normalize(latent_value_rows.astype(jnp.float32)) * (1.0 + scale_vec) + shift_vec
    ).astype(jnp.bfloat16)


def body(
    latents,
    context,
    cond,
    ctx_cond,
    mod_weight,
    query_weight,
    key_matrix,
    value_matrix,
    out_weight,
    query_gain,
    key_gain,
):
    model_width = latents.shape[1]
    head_dim = query_gain.shape[0]
    sp_count = lax.axis_size("sp")
    partials = jnp.dot(
        jax.nn.silu(jnp.stack([cond, ctx_cond])), mod_weight, precision=lax.Precision.HIGHEST
    )
    summed = lax.psum(partials, "sp")
    modulation = lax.all_gather(summed, "tp", axis=1, tiled=True)
    gate_vec = modulation[0, 2 * model_width :]
    normalised_rows = modulate(latents, modulation[0])
    prefix_normalised = modulate(context, modulation[1])
    query_cols = query_weight.shape[1]
    key_cols = key_matrix.shape[1]
    piece = lax.all_gather(normalised_rows, "tp", axis=0, tiled=True)
    projected = jnp.concatenate(
        [
            jnp.dot(piece, query_weight, preferred_element_type=jnp.float32),
            jnp.dot(piece, key_matrix, preferred_element_type=jnp.float32),
            jnp.dot(piece, value_matrix, preferred_element_type=jnp.float32),
        ],
        axis=1,
    )
    row_count = projected.shape[0]
    positions = lax.axis_index("sp") * row_count + jnp.arange(row_count, dtype=jnp.int32)
    query_heads = projected[:, :query_cols].reshape(row_count, -1, head_dim)
    query_heads = axial(normalize(query_heads) * query_gain, positions).astype(jnp.bfloat16)
    key_heads = projected[:, query_cols : query_cols + key_cols].reshape(row_count, -1, head_dim)
    key_heads = axial(normalize(key_heads) * key_gain, positions).astype(jnp.bfloat16)
    value_heads = (
        projected[:, query_cols + key_cols :].reshape(row_count, -1, head_dim).astype(jnp.bfloat16)
    )
    key_part = jnp.dot(prefix_normalised, key_matrix, preferred_element_type=jnp.float32).reshape(
        prefix_normalised.shape[0], -1, head_dim
    )
    value_part = jnp.dot(
        prefix_normalised, value_matrix, preferred_element_type=jnp.float32
    ).reshape(prefix_normalised.shape[0], -1, head_dim)
    local_keys = (normalize(key_part) * key_gain).astype(jnp.bfloat16)
    local_values = value_part.astype(jnp.bfloat16)
    prefix_keys, prefix_values = (
        lax.all_gather(local_keys, "sp", axis=0, tiled=True),
        lax.all_gather(local_values, "sp", axis=0, tiled=True),
    )
    kv_local = key_heads.shape[1]
    group_size = query_heads.shape[1] // kv_local
    grouped = query_heads.reshape(row_count, kv_local, group_size, head_dim).transpose(1, 2, 0, 3)
    grouped = grouped.reshape(kv_local, group_size * row_count, head_dim)
    inv_root = head_dim ** (-0.5)
    lift = math.log(sp_count * row_count / (2.0 * prefix_keys.shape[0]))
    ctx_scores = (
        jnp.einsum("hqd,khd->hqk", grouped, prefix_keys, preferred_element_type=jnp.float32)
        * inv_root
        + lift
    )
    top_init = jnp.max(ctx_scores, axis=-1)
    ctx_weights = jnp.exp(ctx_scores - top_init[..., None])
    initial = (
        top_init,
        jnp.sum(ctx_weights, axis=-1),
        jnp.einsum(
            "hqk,khd->hqd",
            ctx_weights.astype(jnp.bfloat16),
            prefix_values,
            preferred_element_type=jnp.float32,
        ),
    )

    def update(state_now, key_block, value_block):
        top_old, total_old, acc_old = state_now
        scores = (
            jnp.einsum("hqd,khd->hqk", grouped, key_block, preferred_element_type=jnp.float32)
            * inv_root
        )
        top_new = jnp.maximum(top_old, jnp.max(scores, axis=-1))
        factor = jnp.exp(top_old - top_new)
        weights_now = jnp.exp(scores - top_new[..., None])
        acc_new = acc_old * factor[..., None] + jnp.einsum(
            "hqk,khd->hqd",
            weights_now.astype(jnp.bfloat16),
            value_block,
            preferred_element_type=jnp.float32,
        )
        return (top_new, total_old * factor + jnp.sum(weights_now, axis=-1), acc_new)

    key_piece = lax.all_gather(key_heads, "sp", axis=0, tiled=True)
    value_piece = lax.all_gather(value_heads, "sp", axis=0, tiled=True)
    key_count = key_piece.shape[0]
    rows_per_block = math.gcd(key_count, 2048)
    block_count = key_count // rows_per_block
    key_blocks = key_piece.reshape(block_count, rows_per_block, kv_local, head_dim)
    value_blocks = value_piece.reshape(block_count, rows_per_block, kv_local, head_dim)

    def one_step(state_in, blocks_in):
        return (update(state_in, blocks_in[0], blocks_in[1]), None)

    state_out, _ = lax.scan(one_step, initial, (key_blocks, value_blocks))
    top_fin, total_fin, acc_fin = state_out
    attended = (acc_fin / total_fin[..., None]).astype(jnp.bfloat16)
    attended = (
        attended.reshape(kv_local, group_size, row_count, head_dim)
        .transpose(2, 0, 1, 3)
        .reshape(row_count, -1)
    )
    mixed_rows = lax.psum_scatter(
        jnp.dot(attended, out_weight, preferred_element_type=jnp.float32).astype(jnp.bfloat16),
        "tp",
        scatter_dimension=0,
        tiled=True,
    ).astype(jnp.float32)
    return (latents.astype(jnp.float32) + gate_vec * normalize(mixed_rows)).astype(jnp.bfloat16)


def solution(mesh):
    placed = (
        P(("sp", "tp"), None),
        P("sp", None),
        P("sp"),
        P("sp"),
        P("sp", "tp"),
        P(None, "tp"),
        P(None, "tp"),
        P(None, "tp"),
        P("tp", None),
        P(),
        P(),
    )
    return jax.shard_map(
        body, mesh=mesh, in_specs=placed, out_specs=P(("sp", "tp"), None), check_vma=False
    )
```

profile of v0, /device:TPU:0, one launch (start us, length us, event | category | flops | bytes accessed | tf_op | source)
XLA Modules:
  0.0 286.1 jit_solution(9915169423210026204)
XLA Ops:
  6.5 2.4 fusion.41
  9.0 38.8 %psum.7 = f32[2,1536]{1,0:T(2,128)S(1)} all-reduce(f32[2,1536]{1,0:T(2,128)S(1)} %fusion.41), channel_id=1, replica_groups=mesh['sp'=8,'tp'=4] {'sp'}, use_global_device_ids=true, to_apply=%region_0.1 | all-reduce | flops 3072 | bytes 24576 | tf_op jit(solution)/shard_map/psum | solution.py:72
  47.8 5.2 %all_gather.18 = f32[2,6144]{1,0:T(2,128)S(1)} all-gather(f32[2,1536]{1,0:T(2,128)S(1)} %psum.7), channel_id=1, replica_groups=mesh['sp'=8,'tp'=4] {'tp'}, dimensions={1}, use_global_device_ids=true | all-gather | bytes 61440 | tf_op jit(solution)/shard_map/all_gather | solution.py:73
  54.9 2.1 fusion.30
  59.6 17.4 %all-gather.4.cloned.1.call-done = bf16[512,2048]{1,0:T(8,128)(2,1)} async-done(((bf16[128,2048]{1,0:T(8,128)(2,1)}), bf16[512,2048]{1,0:T(8,128)(2,1)}) %all-gather.4.cloned.1.call-update) | async-done | bytes 2097168 | tf_op jit(solution)/shard_map/all_gather | solution.py:79
  77.0 4.0 %multiply_reduce_fusion.1 = (f32[512,2]{0,1:T(2,128)}, f32[512,256]{0,1:T(8,128)}) fusion(bf16[512,2048]{1,0:T(8,128)(2,1)} %all-gather.4.cloned.1.call-done, bf16[2048,256]{1,0:T(8,128)(2,1)} %param.19), kind=kOutput, calls=%fused_computation.57 | convolution fusion | flops 537132032 | bytes 3674112 | tf_op jit(solution)/shard_map/dot_general | solution.py:83
  87.3 3.3 %convolution_convert_fusion.1 = bf16[512,256]{0,1:T(8,128)(2,1)} fusion(bf16[512,2048]{1,0:T(8,128)(2,1)} %all-gather.4.cloned.1.call-done, bf16[2048,256]{1,0:T(8,128)(2,1)} %param.20), kind=kOutput, calls=%fused_computation.32 | convolution fusion | flops 537001984 | bytes 3407872 | tf_op jit(solution)/shard_map/dot_general | solution.py:84
  98.4 31.6 %all_gather.20 = bf16[512,2,128]{2,0,1:T(8,128)(2,1)S(1)} all-gather(bf16[64,2,128]{2,0,1:T(8,128)(2,1)S(1)} %fusion.37), channel_id=1, replica_groups=mesh['sp'=8,'tp'=4] {'sp'}, dimensions={0}, use_global_device_ids=true | all-gather | bytes 294912 | tf_op jit(solution)/shard_map/all_gather | solution.py:106
  129.9 33.5 %all_gather.21 = bf16[512,2,128]{2,0,1:T(8,128)(2,1)} all-gather(bf16[64,2,128]{2,0,1:T(8,128)(2,1)S(1)} %bitcast.103), channel_id=1, replica_groups=mesh['sp'=8,'tp'=4] {'sp'}, dimensions={0}, use_global_device_ids=true | all-gather | bytes 294912 | tf_op jit(solution)/shard_map/all_gather | solution.py:107
  163.5 3.6 %multiply_reduce_fusion = (f32[512,4]{0,1:T(4,128)S(1)}, f32[512,512]{0,1:T(8,128)S(1)}) fusion(bf16[512,2048]{1,0:T(8,128)(2,1)} %all-gather.4.cloned.1.call-done, bf16[2048,512]{1,0:T(8,128)(2,1)} %param.18), kind=kOutput, calls=%fused_computation.44 | convolution fusion | flops 1074264064 | bytes 5251072 | tf_op jit(solution)/shard_map/dot_general | solution.py:82
  169.6 1.9 copy.74
  171.5 1.9 copy.75
  173.5 1.9 pad_maximum_fusion
  179.0 10.1 %all-gather.8.cloned.1.call-done = bf16[4096,2,128]{2,0,1:T(8,128)(2,1)} async-done(((bf16[512,2,128]{2,0,1:T(8,128)(2,1)}), bf16[4096,2,128]{2,0,1:T(8,128)(2,1)}) %all-gather.8.cloned.1.call-update) | async-done | bytes 2097168 | tf_op jit(solution)/shard_map/all_gather | solution.py:151
  189.1 52.1 %while.14 = (s32[]{:T(128)}, f32[2,1024]{1,0:T(2,128)S(1)}, f32[2,1024]{1,0:T(2,128)S(1)}, f32[2,1024,128]{2,1,0:T(8,128)S(1)}, bf16[2,2048,2,128]{3,1,0,2:T(8,1...) while((s32[]{:T(128)}, f32[2,1024]{1,0:T(2,128)S(1)}, ...), condition=%wide.region_11.12_spmd, body=%wide.region_8.11_spmd.sunk | while | flops 2181566464 | bytes 55182420 | solution.py:161
  189.1 9.4 %bitcast_reduce_fusion.2 = (f32[2,1024]{1,0:T(2,128)S(1)}, f32[2,2048,1024]{2,1,0:T(8,128)}) fusion(bf16[2,1024,128]{2,1,0:T(8,128)(2,1)} %get-tuple-element.194, bf16[2,2048,2,128]{3,1,0,2:T(8,128)(2,1)} %get-tuple-element.193, s32[]{:T(128)} %get-tuple-element.181), kind=kOutput, calls=%fused_computation.1.clone.1 | convolution fusion | flops 1082128384 | bytes 18358784 | tf_op jit(solution)/shard_map/while/body/eval_jaxpr/hqd,khd->hqk/dot_general | solution.py:136
  198.5 8.5 %fusion.80 = f32[2,1024]{1,0:T(2,128)S(1)} fusion(f32[2,2048,1024]{2,1,0:T(8,128)} %get-tuple-element.170, f32[2,1024]{1,0:T(2,128)S(1)} %max.4), kind=kLoop, calls=%fused_computation.4.clone.1 | loop fusion | flops 12580864 | bytes 16793600 | tf_op jit(solution)/shard_map/while/body/eval_jaxpr/reduce_sum | solution.py:148
  207.0 8.1 %fusion.81 = f32[2,1024,128]{2,1,0:T(8,128)S(1)} fusion(f32[2,2048,1024]{2,1,0:T(8,128)} %get-tuple-element.170, f32[2,1024]{1,0:T(2,128)S(1)} %max.4, bf16[2,2048,2,128]{3,1,0,2:T(8,128)(2,1)} %get-tuple-element.195, s32[]{:T(128)} %get-tuple-element.181, f32[2,1024,128]{2,1,0:T(8,128)S(1)} %get-tuple-element.184, f32[2,1024]{1,0:T(2,128)S(1)} %get-tuple-element.172), kind=kOutput, calls=%fused_computation.6.clone.1 | convolution fusion | flops 1086849024 | bytes 19939840 | tf_op jit(solution)/shard_map/while/body/eval_jaxpr/hqk,khd->hqd/dot_general | solution.py:142
  215.1 9.4 %bitcast_reduce_fusion.2 = (f32[2,1024]{1,0:T(2,128)S(1)}, f32[2,2048,1024]{2,1,0:T(8,128)}) fusion(bf16[2,1024,128]{2,1,0:T(8,128)(2,1)} %get-tuple-element.194, bf16[2,2048,2,128]{3,1,0,2:T(8,128)(2,1)} %get-tuple-element.193, s32[]{:T(128)} %get-tuple-element.181), kind=kOutput, calls=%fused_computation.1.clone.1 | convolution fusion | flops 1082128384 | bytes 18358784 | tf_op jit(solution)/shard_map/while/body/eval_jaxpr/hqd,khd->hqk/dot_general | solution.py:136
  224.5 8.5 %fusion.80 = f32[2,1024]{1,0:T(2,128)S(1)} fusion(f32[2,2048,1024]{2,1,0:T(8,128)} %get-tuple-element.170, f32[2,1024]{1,0:T(2,128)S(1)} %max.4), kind=kLoop, calls=%fused_computation.4.clone.1 | loop fusion | flops 12580864 | bytes 16793600 | tf_op jit(solution)/shard_map/while/body/eval_jaxpr/reduce_sum | solution.py:148
  233.1 8.1 %fusion.81 = f32[2,1024,128]{2,1,0:T(8,128)S(1)} fusion(f32[2,2048,1024]{2,1,0:T(8,128)} %get-tuple-element.170, f32[2,1024]{1,0:T(2,128)S(1)} %max.4, bf16[2,2048,2,128]{3,1,0,2:T(8,128)(2,1)} %get-tuple-element.195, s32[]{:T(128)} %get-tuple-element.181, f32[2,1024,128]{2,1,0:T(8,128)S(1)} %get-tuple-element.184, f32[2,1024]{1,0:T(2,128)S(1)} %get-tuple-element.172), kind=kOutput, calls=%fused_computation.6.clone.1 | convolution fusion | flops 1086849024 | bytes 19939840 | tf_op jit(solution)/shard_map/while/body/eval_jaxpr/hqk,khd->hqd/dot_general | solution.py:142
  243.6 2.6 convolution_convert_fusion
  246.3 29.9 %reduce-scatter.2.cloned.1.call-done = bf16[128,2048]{1,0:T(8,128)(2,1)} async-done(((bf16[512,2048]{1,0:T(8,128)(2,1)}), bf16[128,2048]{1,0:T(8,128)(2,1)}) %reduce-scatter.2.cloned.1.call-update) | async-done | bytes 524304 | tf_op jit(solution)/shard_map/reduce_scatter | solution.py:169
  277.4 2.1 fusion.31
  (79 shorter events, 28.3 us)
Async XLA Ops:
  6.5 237.1 %copy-start = (bf16[512,2048]{1,0:T(8,128)(2,1)S(1)}, bf16[512,2048]{1,0:T(8,128)(2,1)}, u32[]{:S(2)}) copy-start(bf16[512,2048]{1,0:T(8,128)(2,1)} %param.21) | copy-start | bytes 6291460
  6.5 70.5 %all-gather.4.cloned.1.call-start = ((), (), s32[]{:S(2)}) async-start(), calls=%async_computation.1 | async-start | bytes 2621440 | tf_op jit(solution)/shard_map/all_gather | solution.py:79
  57.0 122.0 %all-gather.6.cloned.1.call-start = ((), (), s32[]{:S(2)}) async-start(), calls=%async_computation.2 | async-start | bytes 2359296 | tf_op jit(solution)/shard_map/all_gather | solution.py:150
  57.6 19.4 %copy-start.6 = (f32[512,32]{0,1:T(8,128)}, f32[512,32]{0,1:T(8,128)S(1)}, u32[]{:S(2)}) copy-start(f32[512,32]{0,1:T(8,128)S(1)} %get-tuple-element.112) | copy-start | bytes 196612
  57.6 19.4 %copy-start.8 = (f32[512,32]{0,1:T(8,128)}, f32[512,32]{0,1:T(8,128)S(1)}, u32[]{:S(2)}) copy-start(f32[512,32]{0,1:T(8,128)S(1)} %get-tuple-element.113) | copy-start | bytes 196612
  81.0 5.5 %copy-start.3 = (bf16[64,2048]{1,0:T(8,128)(2,1)S(1)}, bf16[64,2048]{1,0:T(8,128)(2,1)}, u32[]{:S(2)}) copy-start(bf16[64,2048]{1,0:T(8,128)(2,1)} %param.14) | copy-start | bytes 786436
  85.3 8.4 %copy-start.4 = (bf16[2048,256]{1,0:T(8,128)(2,1)S(1)}, bf16[2048,256]{1,0:T(8,128)(2,1)}, u32[]{:S(2)}) copy-start(bf16[2048,256]{1,0:T(8,128)(2,1)} %param.19) | copy-start | bytes 3145732
  86.5 102.6 %all-gather.8.cloned.1.call-start = ((), (), s32[]{:S(2)}) async-start(), calls=%async_computation.3 | async-start | bytes 2359296 | tf_op jit(solution)/shard_map/all_gather | solution.py:151
  92.4 183.8 %reduce-scatter.2.cloned.1.call-start = ((), (), s32[]{:S(2)}) async-start(), calls=%async_computation.4 | async-start | bytes 2621440 | tf_op jit(solution)/shard_map/reduce_scatter | solution.py:169
  93.1 0.6 copy-start.11
  163.4 3.6 %copy-start.12 = (f32[128]{0:T(128)S(1)}, f32[128]{0:T(128)}, u32[]{:S(2)}) copy-start(f32[128]{0:T(128)} %param.22) | copy-start | bytes 1540
  163.4 3.8 %copy-start.7 = (f32[512,32]{0,1:T(8,128)S(1)}, f32[512,32]{0,1:T(8,128)}, u32[]{:S(2)}) copy-start(f32[512,32]{0,1:T(8,128)} %copy-done.6) | copy-start | bytes 196612
  163.4 3.8 %copy-start.9 = (f32[512,32]{0,1:T(8,128)S(1)}, f32[512,32]{0,1:T(8,128)}, u32[]{:S(2)}) copy-start(f32[512,32]{0,1:T(8,128)} %copy-done.8) | copy-start | bytes 196612
  175.3 0.8 copy-start.1
  176.1 1.6 copy-start.5
  243.6 33.8 %copy-start.2 = (bf16[128,2048]{1,0:T(8,128)(2,1)S(1)}, bf16[128,2048]{1,0:T(8,128)(2,1)}, u32[]{:S(2)}) copy-start(bf16[128,2048]{1,0:T(8,128)(2,1)} %param.13) | copy-start | bytes 1572868
  243.6 33.8 %copy-start.10 = (f32[1,2048]{1,0:T(1,128)S(1)}, f32[1,2048]{1,0:T(1,128)}, u32[]{:S(2)}) copy-start(f32[1,2048]{1,0:T(1,128)} %get-tuple-element.103) | copy-start | bytes 24580
Sparse Core Ops, SparseCore 0:
  57.1 19.8 all-gather.3
  86.6 52.3 all-gather.5
  141.2 47.7 all-gather.7
  246.4 29.7 reduce-scatter.1
where the time goes:
time: 287 us; the launch traced here: 286 us
  blocking collectives  109 us (38%)
  waiting for transfers between devices  57.5 us (20%)
  matrix products  55.5 us (19%)
  other arithmetic  36.5 us (13%)
  local copies, waits for them, and re-layouts  13.9 us (5%)
  between operations  13.4 us (5%)
    psum x1, blocking collectives, body(): summed = lax.psum(partials, 'sp')  38.8 us
    all_gather x1, blocking collectives, body(): lax.all_gather(local_values, 'sp', axis=0, tiled=True)  33.5 us
    all_gather x1, blocking collectives, body(): lax.all_gather(local_keys, 'sp', axis=0, tiled=True)  31.6 us
    reduce_scatter x1, waiting for transfers between devices, body(): lax.psum_scatter(jnp.dot(attended, out_weight, preferred_element_type=jnp...  29.9 us
    dot_general x2, matrix products, update(): jnp.einsum('hqd,khd->hqk', grouped, key_block, preferred_element_type=jnp...  18.8 us
    all_gather x1, waiting for transfers between devices, body(): piece = lax.all_gather(normalised_rows, 'tp', axis=0, tiled=True)  17.4 us
    reduce_sum x2, other arithmetic, update(): jnp.sum(weights_now, axis=-1)  17 us
    dot_general x2, matrix products, update(): jnp.einsum('hqk,khd->hqd', weights_now.astype(jnp.bfloat16), value_block,...  16.2 us
  transfers between devices with their start and end apart: 4, of which 3 were waited for; matrix products, arithmetic and copies ran while one was open for 10% of the time, Pallas kernels for 0%

commit v1 on v0

v1 whole, which is shorter than its diff:
```python
import functools
import math

import jax
import jax.numpy as jnp
from jax import lax
from jax.experimental import pallas as pl
from jax.experimental.pallas import tpu as pltpu
from jax.sharding import PartitionSpec as P

GRID_W = 64
NORM_EPS = 1e-06
ROPE_BASE = 10000.0
MESH = pl.DeviceIdType.MESH
BF16 = jnp.bfloat16
F32 = jnp.float32


def row_size(sp_count):
    size = 1
    while 4 * size * size <= sp_count:
        size *= 2
    return size


def tables(positions, head_dim):
    quarter = head_dim // 4
    inv_freq = ROPE_BASE ** (-jnp.arange(quarter, dtype=F32) / quarter)
    row_ang = inv_freq[:, None] * (positions // GRID_W).astype(F32)[None, :]
    col_ang = inv_freq[:, None] * (positions % GRID_W).astype(F32)[None, :]
    cos = jnp.concatenate([jnp.cos(row_ang)] * 2 + [jnp.cos(col_ang)] * 2, axis=0)
    row_sin, col_sin = jnp.sin(row_ang), jnp.sin(col_ang)
    sin = jnp.concatenate([-row_sin, row_sin, -col_sin, col_sin], axis=0)
    return cos, sin


def remote(src, dst, send, recv, dev):
    return pltpu.make_async_remote_copy(
        src_ref=src, dst_ref=dst, send_sem=send, recv_sem=recv, device_id=dev, device_id_type=MESH
    )


def front_kernel(
    sp_count, tp_count, head_dim,
    cond_ref, mw_hbm, lat_hbm, ctx_ref, wq_hbm, wk_hbm, wv_hbm, qg_ref, kg_ref, cos_ref, sin_ref,
    qt_ref, k_ref, vt_ref, ck_ref, cv_ref, gate_ref,
    mw, lat, wq, wk, wv, part, tot, mod, xn, load_sem,
    lat_send, lat_recv, part_send, part_recv, tot_send, tot_recv,
):
    s, t = lax.axis_index("sp"), lax.axis_index("tp")
    y, c = t // 2, t % 2
    y_count = tp_count // 2
    partner = y * 2 + 1 - c
    rows = lat.shape[1]
    width = lat.shape[2]
    model_cols = mod.shape[1]

    own = pltpu.make_async_copy(lat_hbm, lat.at[t], load_sem.at[0])
    own.start()
    loads = [
        pltpu.make_async_copy(a, b, load_sem.at[1 + i])
        for i, (a, b) in enumerate(((mw_hbm, mw), (wq_hbm, wq), (wk_hbm, wk), (wv_hbm, wv)))
    ]
    for one in loads:
        one.start()

    barrier = pltpu.get_barrier_semaphore()
    for j in range(1, sp_count):
        pl.semaphore_signal(barrier, inc=1, device_id=((s + j) % sp_count, t), device_id_type=MESH)
    for j in range(1, tp_count):
        pl.semaphore_signal(barrier, inc=1, device_id=(s, (t + j) % tp_count), device_id_type=MESH)
    pl.semaphore_wait(barrier, sp_count + tp_count - 2)

    own.wait()
    sends = []
    for j in range(1, y_count):
        peer = ((y + j) % y_count) * 2 + c
        sends.append(remote(lat.at[t], lat.at[t], lat_send.at[j], lat_recv.at[t], (s, peer)))
    sends.append(remote(lat.at[t], lat.at[t], lat_send.at[0], lat_recv.at[t], (s, partner)))
    for one in sends:
        one.start()

    loads[0].wait()
    cond = cond_ref[...]
    cond = cond * jax.nn.sigmoid(cond)
    part[s] = jnp.dot(
        cond, mw[...], precision=lax.Precision.HIGHEST, preferred_element_type=F32
    )[:2]
    more = [
        remote(part.at[s], part.at[s], part_send.at[j], part_recv.at[s], ((s + j) % sp_count, t))
        for j in range(1, sp_count)
    ]
    for one in more:
        one.start()
    for j in range(1, sp_count):
        src = (s + j) % sp_count
        remote(part.at[src], part.at[src], part_send.at[0], part_recv.at[src], (s, t)).wait_recv()
    total = part[0]
    for j in range(1, sp_count):
        total = total + part[j]
    tot[t] = total
    last = [
        remote(tot.at[t], tot.at[t], tot_send.at[j], tot_recv.at[t], (s, (t + j) % tp_count))
        for j in range(1, tp_count)
    ]
    for one in last:
        one.start()
    for j in range(1, tp_count):
        src = (t + j) % tp_count
        remote(tot.at[src], tot.at[src], tot_send.at[0], tot_recv.at[src], (s, t)).wait_recv()
    cols = model_cols // tp_count
    for j in range(tp_count):
        mod[:, j * cols : (j + 1) * cols] = tot[j]
    gate_ref[...] = mod[0:1, 2 * width :]

    def modulate(x, r):
        x = x.astype(F32)
        scaled = x * lax.rsqrt(jnp.mean(x * x, axis=-1, keepdims=True) + NORM_EPS)
        shift, scale = mod[r : r + 1, :width], mod[r : r + 1, width : 2 * width]
        return (scaled * (1.0 + scale) + shift).astype(BF16)

    for one in loads[1:]:
        one.wait()

    cn = modulate(ctx_ref[...], 1)
    kc = jnp.dot(cn, wk[...], preferred_element_type=F32)
    vc = jnp.dot(cn, wv[...], preferred_element_type=F32)
    for h in range(kc.shape[1] // head_dim):
        kh = kc[:, h * head_dim : (h + 1) * head_dim]
        kh = kh * lax.rsqrt(jnp.mean(kh * kh, axis=-1, keepdims=True) + NORM_EPS) * kg_ref[...]
        ck_ref[h] = kh.astype(BF16)
        cv_ref[h] = vc[:, h * head_dim : (h + 1) * head_dim].astype(BF16)

    q4 = head_dim // 4
    qgain, kgain = qg_ref[...], kg_ref[...]

    def turn(yt, cos, sin):
        part_t = jnp.concatenate(
            [yt[q4 : 2 * q4], yt[:q4], yt[3 * q4 :], yt[2 * q4 : 3 * q4]], axis=0
        )
        return yt * cos + part_t * sin

    def unit(yh, gain):
        return yh * lax.rsqrt(jnp.mean(yh * yh, axis=-1, keepdims=True) + NORM_EPS) * gain

    span = 2 * rows
    relays = []
    for j in range(y_count):
        yy = (y + j) % y_count
        if j > 0:
            src = yy * 2 + c
            remote(lat.at[src], lat.at[src], lat_send.at[0], lat_recv.at[src], (s, t)).wait_recv()
            one = remote(
                lat.at[src], lat.at[src], lat_send.at[y_count - 1 + j], lat_recv.at[src], (s, partner)
            )
            one.start()
            relays.append(one)
        other = yy * 2 + 1 - c
        remote(lat.at[other], lat.at[other], lat_send.at[0], lat_recv.at[other], (s, t)).wait_recv()
        for i in range(2):
            xn[i * rows : (i + 1) * rows, :] = modulate(lat[yy * 2 + i], 0)
        x = xn[...]
        at = pl.ds(pl.multiple_of(yy * span, span), span)
        cos, sin = cos_ref[:, at], sin_ref[:, at]
        for w, kind in ((wq, 0), (wk, 1), (wv, 2)):
            step = min(2 * head_dim, w.shape[1])
            for n in range(0, w.shape[1], step):
                full = jnp.dot(x, w[:, n : n + step], preferred_element_type=F32)
                for m in range(0, step, head_dim):
                    h = (n + m) // head_dim
                    yh = full[:, m : m + head_dim]
                    if kind == 0:
                        qt_ref[h, :, at] = turn(unit(yh, qgain).T, cos, sin).astype(BF16)
                    elif kind == 1:
                        k_ref[h, at, :] = turn(unit(yh, kgain).T, cos, sin).T.astype(BF16)
                    else:
                        vt_ref[h, :, at] = yh.T.astype(BF16)
    for one in sends + more + last + relays:
        one.wait_send()


def attend_kernel(
    sp_count, x_count, group, lift,
    k_hbm, vt_hbm, ck_hbm, cv_hbm, qt_ref,
    out_ref,
    kb, vb, cb, top, tot, acc, load_sem, send_sem, recv_sem,
):
    s, t = lax.axis_index("sp"), lax.axis_index("tp")
    z, x = s // x_count, s % x_count
    z_count = sp_count // x_count
    heads, head_dim, rows = qt_ref.shape
    kv_heads = heads // group
    factor = head_dim ** (-0.5) * math.log2(math.e)

    loads = [
        pltpu.make_async_copy(a, b, load_sem.at[i])
        for i, (a, b) in enumerate(
            (
                (ck_hbm, cb.at[s, 0]),
                (cv_hbm, cb.at[s, 1]),
                (k_hbm, kb.at[s]),
                (vt_hbm, vb.at[s]),
            )
        )
    ]
    for one in loads:
        one.start()
    barrier = pltpu.get_barrier_semaphore()
    targets = []
    for sign in (1, -1):
        ok = (z + sign >= 0) & (z + sign < z_count)
        peer = ((z + sign + z_count) % z_count) * x_count + x
        targets.append((ok, peer))
    for ok, peer in targets:

        @pl.when(ok)
        def _():
            pl.semaphore_signal(barrier, inc=1, device_id=(peer, t), device_id_type=MESH)

    for j in range(1, x_count):
        peer = z * x_count + (x + j) % x_count
        pl.semaphore_signal(barrier, inc=1, device_id=(peer, t), device_id_type=MESH)
    ends_here = (z == 0).astype(jnp.int32) + (z == z_count - 1).astype(jnp.int32)
    pl.semaphore_wait(barrier, x_count + 1 - ends_here)

    top[...] = jnp.full_like(top, -1e30)
    tot[...] = jnp.zeros_like(tot)
    acc[...] = jnp.zeros_like(acc)
    for one in loads:
        one.wait()

    bufs = (cb, kb, vb)

    def copies(src, way, peer):
        return [
            remote(b.at[src], b.at[src], send_sem.at[i, src, way], recv_sem.at[i, src], (peer, t))
            for i, b in enumerate(bufs)
        ]

    def source(k):
        low = jnp.minimum(z, z_count - 1 - z)
        both = k <= 2 * low
        dist = jnp.where(both, (k + 1) // 2, k - low)
        up = jnp.where(both, k % 2 == 1, z < z_count - 1 - z)
        return jnp.where(up, z + dist, z - dist)

    def update(i, keys, values_t, bias):
        sc = jnp.dot(keys, qt_ref[i], preferred_element_type=F32) * factor
        if bias != 0.0:
            sc = sc + bias
        old = top[i]
        new = jnp.maximum(old, jnp.max(sc, axis=0, keepdims=True))
        p = jnp.exp2(sc - new)
        f = jnp.exp2(old - new)
        top[i] = new
        tot[i] = tot[i] * f + jnp.sum(p, axis=0, keepdims=True)
        acc[i] = acc[i] * f + jnp.dot(values_t, p.astype(BF16), preferred_element_type=F32)

    def block(src):
        def head(i, carry):
            h = i // group
            update(i, kb[src, h], vb[src, h], 0.0)
            return carry

        lax.fori_loop(0, heads, head, 0)

    def wait_from(src):
        for one in copies(src, 0, s):
            one.wait_recv()

    def step(k, carry):
        zz = source(k)
        src = zz * x_count + x

        @pl.when(k > 0)
        def _():
            wait_from(src)

        for way, (ok, peer) in enumerate(targets):
            mine = zz <= z if way == 0 else zz >= z

            @pl.when(ok & mine)
            def _():
                for one in copies(src, way, peer):
                    one.start()

        for j in range(1, x_count):
            for one in copies(src, 1 + j, z * x_count + (x + j) % x_count):
                one.start()
        block(src)

        @pl.when(k > 0)
        def _():
            before = source(k - 1)
            for j in range(1, x_count):
                old = before * x_count + (x + j) % x_count
                wait_from(old)
                block(old)

        return carry

    lax.fori_loop(0, z_count, step, 0)
    final = source(z_count - 1)
    ends = [final * x_count + (x + j) % x_count for j in range(1, x_count)]
    for src in ends:
        copies(src, 0, s)[0].wait_recv()
    for i in range(heads):
        h = i // group
        keys = jnp.concatenate([cb[j, 0, h] for j in range(sp_count)], axis=0)
        vals = jnp.concatenate([cb[j, 1, h] for j in range(sp_count)], axis=0)
        update(i, keys, vals.astype(F32).T.astype(BF16), lift * math.log2(math.e))
    for src in ends:
        for one in copies(src, 0, s)[1:]:
            one.wait_recv()
        block(src)
    for i in range(heads):
        out_ref[:, i * head_dim : (i + 1) * head_dim] = (acc[i] / tot[i]).T.astype(BF16)

    def drain(k, carry):
        zz = source(k)
        src = zz * x_count + x
        for way, (ok, peer) in enumerate(targets):
            mine = zz <= z if way == 0 else zz >= z

            @pl.when(ok & mine)
            def _():
                for one in copies(src, way, peer):
                    one.wait_send()

        for j in range(1, x_count):
            for one in copies(src, 1 + j, z * x_count + (x + j) % x_count):
                one.wait_send()
        return carry

    lax.fori_loop(0, z_count, drain, 0)


def mix_kernel(
    tp_count, chunks,
    att_ref, wo_ref, lat_ref, gate_ref,
    out_ref,
    core_out, core_in, mesh_out, mesh_in, mixed, core_send, core_recv, mesh_send, mesh_recv,
):
    s, t = lax.axis_index("sp"), lax.axis_index("tp")
    y, c = t // 2, t % 2
    y_count = tp_count // 2
    partner = y * 2 + 1 - c
    rows, width = lat_ref.shape
    step = width // chunks
    barrier = pltpu.get_barrier_semaphore()
    peers = [((y + j) % y_count) * 2 + c for j in range(1, y_count)]
    for peer in peers + [partner]:
        pl.semaphore_signal(barrier, inc=1, device_id=(s, peer), device_id_type=MESH)
    pl.semaphore_wait(barrier, y_count)

    def piece(n, j, cc):
        yy = (y + j) % y_count
        at = pl.ds(pl.multiple_of((yy * 2 + cc) * rows, rows), rows)
        return jnp.dot(
            att_ref[at, :], wo_ref[:, n * step : (n + 1) * step], preferred_element_type=F32
        )

    order = list(range(1, y_count)) + [0]
    cores = [
        remote(core_out.at[n], core_in.at[n], core_send.at[n], core_recv.at[n], (s, partner))
        for n in range(chunks)
    ]
    sent = []
    for n in range(chunks):
        for j in order:
            core_out[n, j] = piece(n, j, 1 - c).astype(BF16)
        cores[n].start()
    for n in range(chunks):
        mine = [piece(n, j, c) for j in order]
        cores[n].wait_recv()
        for j, value in zip(order, mine):
            value = value + core_in[n, j].astype(F32)
            if j == 0:
                mixed[n] = value
            else:
                mesh_out[n, j - 1] = value.astype(BF16)
                one = remote(
                    mesh_out.at[n, j - 1], mesh_in.at[n, j - 1], mesh_send.at[n, j - 1],
                    mesh_recv.at[n, j - 1], (s, peers[j - 1]),
                )
                one.start()
                sent.append(one)
    for one in sent:
        one.wait_recv()
    square = jnp.zeros((rows, 1), F32)
    for n in range(chunks):
        value = mixed[n]
        for j in range(1, y_count):
            value = value + mesh_in[n, j - 1].astype(F32)
        mixed[n] = value
        square = square + jnp.sum(value * value, axis=-1, keepdims=True)
    inv = lax.rsqrt(square / width + NORM_EPS)
    for n in range(chunks):
        at = slice(n * step, (n + 1) * step)
        out_ref[:, at] = (
            lat_ref[:, at].astype(F32) + gate_ref[:, at] * (mixed[n] * inv)
        ).astype(BF16)
    for one in sent + cores:
        one.wait_send()


ANY = pl.BlockSpec(memory_space=pl.ANY)
VM = pl.BlockSpec(memory_space=pltpu.VMEM)
DMA = pltpu.SemaphoreType.DMA


def body(
    latents,
    context,
    cond,
    ctx_cond,
    mod_weight,
    query_weight,
    key_matrix,
    value_matrix,
    out_weight,
    query_gain,
    key_gain,
):
    sp_count, tp_count = lax.axis_size("sp"), lax.axis_size("tp")
    x_count = row_size(sp_count)
    rows, width = latents.shape
    ctx_rows = context.shape[0]
    head_dim = query_gain.shape[0]
    heads = query_weight.shape[1] // head_dim
    kv_heads = key_matrix.shape[1] // head_dim
    all_rows = rows * tp_count
    mod_cols = mod_weight.shape[1]
    positions = lax.axis_index("sp") * all_rows + jnp.arange(all_rows, dtype=jnp.int32)
    cos, sin = tables(positions, head_dim)
    pair = jnp.concatenate(
        [cond[None], ctx_cond[None], jnp.zeros((6, cond.shape[0]), F32)], axis=0
    )
    sds = jax.ShapeDtypeStruct
    qt, k, vt, ck, cv, gate = pl.pallas_call(
        functools.partial(front_kernel, sp_count, tp_count, head_dim),
        out_shape=[
            sds((heads, head_dim, all_rows), BF16),
            sds((kv_heads, all_rows, head_dim), BF16),
            sds((kv_heads, head_dim, all_rows), BF16),
            sds((kv_heads, ctx_rows, head_dim), BF16),
            sds((kv_heads, ctx_rows, head_dim), BF16),
            sds((1, width), F32),
        ],
        in_specs=[VM, ANY, ANY, VM, ANY, ANY, ANY, VM, VM, VM, VM],
        out_specs=[VM] * 6,
        scratch_shapes=[
            pltpu.VMEM(mod_weight.shape, F32),
            pltpu.VMEM((tp_count, rows, width), BF16),
            pltpu.VMEM(query_weight.shape, BF16),
            pltpu.VMEM(key_matrix.shape, BF16),
            pltpu.VMEM(value_matrix.shape, BF16),
            pltpu.VMEM((sp_count, 2, mod_cols), F32),
            pltpu.VMEM((tp_count, 2, mod_cols), F32),
            pltpu.VMEM((2, mod_cols * tp_count), F32),
            pltpu.VMEM((2 * rows, width), BF16),
            DMA((5,)),
            DMA((tp_count,)),
            DMA((tp_count,)),
            DMA((sp_count,)),
            DMA((sp_count,)),
            DMA((tp_count,)),
            DMA((tp_count,)),
        ],
        compiler_params=pltpu.CompilerParams(
            collective_id=0, has_side_effects=True, vmem_limit_bytes=48 << 20
        ),
        name="front",
    )(
        pair, mod_weight, latents, context, query_weight, key_matrix, value_matrix,
        query_gain[None], key_gain[None], cos, sin,
    )

    lift = math.log(sp_count * all_rows / (2.0 * sp_count * ctx_rows))
    att = pl.pallas_call(
        functools.partial(attend_kernel, sp_count, x_count, heads // kv_heads, lift),
        out_shape=sds((all_rows, heads * head_dim), BF16),
        in_specs=[ANY, ANY, ANY, ANY, VM],
        out_specs=VM,
        scratch_shapes=[
            pltpu.VMEM((sp_count, kv_heads, all_rows, head_dim), BF16),
            pltpu.VMEM((sp_count, kv_heads, head_dim, all_rows), BF16),
            pltpu.VMEM((sp_count, 2, kv_heads, ctx_rows, head_dim), BF16),
            pltpu.VMEM((heads, 1, all_rows), F32),
            pltpu.VMEM((heads, 1, all_rows), F32),
            pltpu.VMEM((heads, head_dim, all_rows), F32),
            DMA((4,)),
            DMA((3, sp_count, x_count + 1)),
            DMA((3, sp_count)),
        ],
        compiler_params=pltpu.CompilerParams(
            collective_id=1, has_side_effects=True, vmem_limit_bytes=48 << 20
        ),
        name="attend",
    )(k, vt, ck, cv, qt)

    chunks = 4
    y_count = tp_count // 2
    step = width // chunks
    far = max(y_count - 1, 1)
    return pl.pallas_call(
        functools.partial(mix_kernel, tp_count, chunks),
        out_shape=sds((rows, width), BF16),
        in_specs=[VM] * 4,
        out_specs=VM,
        scratch_shapes=[
            pltpu.VMEM((chunks, y_count, rows, step), BF16),
            pltpu.VMEM((chunks, y_count, rows, step), BF16),
            pltpu.VMEM((chunks, far, rows, step), BF16),
            pltpu.VMEM((chunks, far, rows, step), BF16),
            pltpu.VMEM((chunks, rows, step), F32),
            DMA((chunks,)),
            DMA((chunks,)),
            DMA((chunks, far)),
            DMA((chunks, far)),
        ],
        compiler_params=pltpu.CompilerParams(
            collective_id=2, has_side_effects=True, vmem_limit_bytes=48 << 20
        ),
        name="mix",
    )(att, out_weight, latents, gate)


def solution(mesh):
    placed = (
        P(("sp", "tp"), None),
        P("sp", None),
        P("sp"),
        P("sp"),
        P("sp", "tp"),
        P(None, "tp"),
        P(None, "tp"),
        P(None, "tp"),
        P("tp", None),
        P(),
        P(),
    )
    return jax.shard_map(
        body, mesh=mesh, in_specs=placed, out_specs=P(("sp", "tp"), None), check_vma=False
    )
```

time: 287 us -> 114 us (0.40)
  blocking collectives: 109 us -> 0 us
  Pallas kernels: 0 us -> 104 us
  waiting for transfers between devices: 57.5 us -> 0 us
  matrix products: 55.5 us -> 0 us
  other arithmetic: 36.5 us -> 1.37 us
  between operations: 13.4 us -> 0.08 us
  local copies, waits for them, and re-layouts: 13.9 us -> 8.03 us
    pallas_call x0 -> x3, Pallas kernels: none -> 104 us  [the longest x1 61.3 us: body(): pl.pallas_call(functools.partial(attend_kernel, sp_count, x_count, heads...]
    all_gather x3 -> x0, blocking collectives: 70.3 us -> none  [the longest x1 33.5 us: body(): lax.all_gather(local_values, 'sp', axis=0, tiled=True)]
    dot_general x13 -> x0, matrix products: 55.5 us -> none  [the longest x2 18.8 us: update(): jnp.einsum('hqd,khd->hqk', grouped, key_block, preferred_element_type=jnp...]
    psum x1 -> x0, blocking collectives: 38.8 us -> none  [body(): summed = lax.psum(partials, 'sp')]
    reduce_scatter x1 -> x0, waiting for transfers between devices: 29.9 us -> none  [body(): lax.psum_scatter(jnp.dot(attended, out_weight, preferred_element_type=jnp...]
    all_gather x3 -> x0, waiting for transfers between devices: 27.5 us -> none  [the longest x1 17.4 us: body(): piece = lax.all_gather(normalised_rows, 'tp', axis=0, tiled=True)]
    reduce_sum x7 -> x0, other arithmetic: 21.2 us -> none  [the longest x2 17 us: update(): jnp.sum(weights_now, axis=-1)]
    unnamed x26 -> x19, local copies, waits for them, and re-layouts: 1.42 us -> 7.95 us
  transfers between devices with their start and end apart: 4 -> 0, of which waited for: 3 -> 0; matrix products, arithmetic and copies ran while one was open for 10% -> 0% of each run, Pallas kernels for 0% -> 0%
where the time goes in v1:
time: 114 us
  Pallas kernels  104 us (91%)
  local copies, waits for them, and re-layouts  8.03 us (7%)
  other arithmetic  1.37 us (1%)
    pallas_call x1, Pallas kernels, body(): pl.pallas_call(functools.partial(attend_kernel, sp_count, x_count, heads...  61.3 us
    pallas_call x1, Pallas kernels, body(): pl.pallas_call(functools.partial(front_kernel, sp_count, tp_count, head_d...  26 us
    pallas_call x1, Pallas kernels, body(): pl.pallas_call(functools.partial(mix_kernel, tp_count, chunks), out_shape...  16.8 us
    unnamed x19, local copies, waits for them, and re-layouts  7.95 us

profile of v1, /device:TPU:0, one launch (start us, length us, event | category | flops | bytes accessed | tf_op | source)
XLA Modules:
  0.0 113.6 jit_solution(15217921814885754536)
XLA Ops:
  0.0 0.1 pad.10.clone
  0.1 0.8 maximum_maximum_fusion.cond_ref
  0.9 0.5 fusion
  1.5 0.0 copy-start
  1.5 1.0 copy-done
  2.5 0.0 copy-start.3
  2.5 1.4 %copy-done.3 = f32[256,1536]{1,0:T(8,128)S(1)} copy-done((f32[256,1536]{1,0:T(8,128)S(1)}, f32[256,1536]{1,0:T(8,128)}, u32[]{:S(2)}) %copy-start.3) | copy-done | bytes 1572888
  3.9 0.0 copy-start.4
  3.9 1.2 %copy-done.4 = bf16[2048,256]{1,0:T(8,128)(2,1)S(1)} copy-done((bf16[2048,256]{1,0:T(8,128)(2,1)S(1)}, bf16[2048,256]{1,0:T(8,128)(2,1)}, u32[]{:S(2)}) %copy-start.4) | copy-done | bytes 1048600
  5.2 0.0 copy-start.5
  5.2 1.2 %copy-done.5 = bf16[2048,256]{1,0:T(8,128)(2,1)S(1)} copy-done((bf16[2048,256]{1,0:T(8,128)(2,1)S(1)}, bf16[2048,256]{1,0:T(8,128)(2,1)}, u32[]{:S(2)}) %copy-start.5) | copy-done | bytes 1048600
  6.4 0.0 copy-start.6
  6.4 0.9 copy-done.6
  7.3 0.0 copy-start.7
  7.3 0.7 copy-done.7
  8.0 0.0 copy-start.8
  8.0 0.7 copy-done.8
  8.6 0.0 copy-start.1
  8.6 26.0 %front.1 = (bf16[4,128,512]{2,1,0:T(8,128)(2,1)S(1)}, bf16[2,512,128]{2,1,0:T(8,128)(2,1)S(1)}, bf16[2,128,512]{2,1,0:T(8,128)(2,1)S(1)}, bf16[2,64,128]{2,1,0:T...) custom-call(f32[8,256]{1,0:T(8,128)S(1)} %maximum_maximum_fusion.cond_ref, ...), custom_call_target="tpu_custom_call" | custom-call | tf_op jit(solution)/shard_map/front/pallas_call | solution.py:440
  34.7 61.3 %attend.1.att_ref = bf16[512,512]{1,0:T(8,128)(2,1)S(1)} custom-call(bf16[2,512,128]{2,1,0:T(8,128)(2,1)S(1)} %get-tuple-element.11.k_hbm, bf16[2,128,512]{2,1,0:T(8,128)(2,1)S(1)} %get-tuple-element.12.vt_hbm, bf16[2,64,128]{2,1,0:T(8,128)(2,1)S(1)} %get-tuple-element.13.ck_hbm, bf16[2,64,128]{2,1,0:T(8,128)(2,1)S(1)} %get-tuple-element.14.cv_hbm, ...), custom_call_target="tpu_custom_call" | custom-call | tf_op jit(solution)/shard_map/attend/pallas_call | solution.py:480
  96.0 0.0 copy-done.1
  96.0 0.0 copy-done.2
  96.0 16.8 %mix.1 = bf16[128,2048]{1,0:T(8,128)(2,1)S(1)} custom-call(bf16[512,512]{1,0:T(8,128)(2,1)S(1)} %attend.1.att_ref, bf16[512,2048]{1,0:T(8,128)(2,1)S(1)} %copy-done.2, bf16[128,2048]{1,0:T(8,128)(2,1)S(1)} %copy-done.1, f32[1,2048]{1,0:T(1,128)S(1)} %get-tuple-element.16.gate_ref), custom_call_target="tpu_custom_call" | custom-call | tf_op jit(solution)/shard_map/mix/pallas_call | solution.py:506
  112.8 0.8 copy.13
  (6 shorter events, 0.1 us)
Async XLA Ops:
  1.5 1.0 copy-start
  2.5 1.4 %copy-start.3 = (f32[256,1536]{1,0:T(8,128)S(1)}, f32[256,1536]{1,0:T(8,128)}, u32[]{:S(2)}) copy-start(f32[256,1536]{1,0:T(8,128)} %mw_hbm.1) | copy-start | bytes 4718596
  3.9 1.2 %copy-start.4 = (bf16[2048,256]{1,0:T(8,128)(2,1)S(1)}, bf16[2048,256]{1,0:T(8,128)(2,1)}, u32[]{:S(2)}) copy-start(bf16[2048,256]{1,0:T(8,128)(2,1)} %wk_hbm.1) | copy-start | bytes 3145732
  5.2 1.2 %copy-start.5 = (bf16[2048,256]{1,0:T(8,128)(2,1)S(1)}, bf16[2048,256]{1,0:T(8,128)(2,1)}, u32[]{:S(2)}) copy-start(bf16[2048,256]{1,0:T(8,128)(2,1)} %wv_hbm.1) | copy-start | bytes 3145732
  6.4 0.9 copy-start.6
  7.3 0.7 copy-start.7
  8.0 0.7 copy-start.8
  8.6 87.4 %copy-start.1 = (bf16[128,2048]{1,0:T(8,128)(2,1)S(1)}, bf16[128,2048]{1,0:T(8,128)(2,1)}, u32[]{:S(2)}) copy-start(bf16[128,2048]{1,0:T(8,128)(2,1)} %lat_ref.1) | copy-start | bytes 1572868
  8.6 87.4 %copy-start.2 = (bf16[512,2048]{1,0:T(8,128)(2,1)S(1)}, bf16[512,2048]{1,0:T(8,128)(2,1)}, u32[]{:S(2)}) copy-start(bf16[512,2048]{1,0:T(8,128)(2,1)} %wo_ref.1) | copy-start | bytes 6291460

commit v2 on v1

--- a/solution.py
+++ b/solution.py
@@ -14,6 +14,7 @@
 MESH = pl.DeviceIdType.MESH
 BF16 = jnp.bfloat16
 F32 = jnp.float32
+VMEM_BYTES = 67043328
 
 
 def row_size(sp_count):
@@ -43,7 +44,7 @@
 def front_kernel(
     sp_count, tp_count, head_dim,
     cond_ref, mw_hbm, lat_hbm, ctx_ref, wq_hbm, wk_hbm, wv_hbm, qg_ref, kg_ref, cos_ref, sin_ref,
-    qt_ref, k_ref, vt_ref, ck_ref, cv_ref, gate_ref,
+    qt_ref, k_ref, vt_ref, ckv_ref, gate_ref,
     mw, lat, wq, wk, wv, part, tot, mod, xn, load_sem,
     lat_send, lat_recv, part_send, part_recv, tot_send, tot_recv,
 ):
@@ -128,8 +129,8 @@
     for h in range(kc.shape[1] // head_dim):
         kh = kc[:, h * head_dim : (h + 1) * head_dim]
         kh = kh * lax.rsqrt(jnp.mean(kh * kh, axis=-1, keepdims=True) + NORM_EPS) * kg_ref[...]
-        ck_ref[h] = kh.astype(BF16)
-        cv_ref[h] = vc[:, h * head_dim : (h + 1) * head_dim].astype(BF16)
+        ckv_ref[h, 0] = kh.astype(BF16)
+        ckv_ref[h, 1] = vc[:, h * head_dim : (h + 1) * head_dim].astype(BF16)
 
     q4 = head_dim // 4
     qgain, kgain = qg_ref[...], kg_ref[...]
@@ -181,7 +182,7 @@
 
 def attend_kernel(
     sp_count, x_count, group, lift,
-    k_hbm, vt_hbm, ck_hbm, cv_hbm, qt_ref,
+    k_hbm, vt_hbm, ckv_hbm, qt_ref,
     out_ref,
     kb, vb, cb, top, tot, acc, load_sem, send_sem, recv_sem,
 ):
@@ -196,8 +197,7 @@
         pltpu.make_async_copy(a, b, load_sem.at[i])
         for i, (a, b) in enumerate(
             (
-                (ck_hbm, cb.at[s, 0]),
-                (cv_hbm, cb.at[s, 1]),
+                (ckv_hbm, cb.at[s]),
                 (k_hbm, kb.at[s]),
                 (vt_hbm, vb.at[s]),
             )
@@ -306,8 +306,8 @@
         copies(src, 0, s)[0].wait_recv()
     for i in range(heads):
         h = i // group
-        keys = jnp.concatenate([cb[j, 0, h] for j in range(sp_count)], axis=0)
-        vals = jnp.concatenate([cb[j, 1, h] for j in range(sp_count)], axis=0)
+        keys = jnp.concatenate([cb[j, h, 0] for j in range(sp_count)], axis=0)
+        vals = jnp.concatenate([cb[j, h, 1] for j in range(sp_count)], axis=0)
         update(i, keys, vals.astype(F32).T.astype(BF16), lift * math.log2(math.e))
     for src in ends:
         for one in copies(src, 0, s)[1:]:
@@ -333,6 +333,173 @@
         return carry
 
     lax.fori_loop(0, z_count, drain, 0)
+
+
+def pair_kernel(
+    sp_count, x_count, group, lift,
+    k_hbm, vt_hbm, ckv_hbm, qt_ref,
+    out_ref,
+    kb, vb, cb, top, tot, acc, load_sem, qb, ab, send_sem, recv_sem, swap_sem,
+):
+    s, t = lax.axis_index("sp"), lax.axis_index("tp")
+    z, x = s // x_count, s % x_count
+    z_count = sp_count // x_count
+    heads, head_dim, rows = qt_ref.shape
+    factor = head_dim ** (-0.5) * math.log2(math.e)
+    mine = z % 2
+    mate = (z + 1 - 2 * mine) * x_count + x
+
+    bufs = (cb, kb, vb)
+    loads = [
+        pltpu.make_async_copy(a, b.at[s], load_sem.at[i])
+        for i, (a, b) in enumerate(zip((ckv_hbm, k_hbm, vt_hbm), bufs))
+    ]
+    for one in loads:
+        one.start()
+    barrier = pltpu.get_barrier_semaphore()
+    targets = []
+    for sign in (1, -1):
+        ok = (z + sign >= 0) & (z + sign < z_count)
+        peer = ((z + sign + z_count) % z_count) * x_count + x
+        targets.append((ok, peer))
+
+        @pl.when(ok)
+        def _():
+            pl.semaphore_signal(barrier, inc=1, device_id=(peer, t), device_id_type=MESH)
+
+    for j in range(1, x_count):
+        peer = z * x_count + (x + j) % x_count
+        pl.semaphore_signal(barrier, inc=1, device_id=(peer, t), device_id_type=MESH)
+    ends_here = (z == 0).astype(jnp.int32) + (z == z_count - 1).astype(jnp.int32)
+    pl.semaphore_wait(barrier, x_count + 1 - ends_here)
+
+    swap_q = remote(
+        qt_ref.at[pl.ds((1 - mine) * group, group)], qb.at[0],
+        swap_sem.at[0], swap_sem.at[1], (mate, t),
+    )
+    swap_q.start()
+    qb[1] = qt_ref[pl.ds(mine * group, group)]
+    top[...] = jnp.full_like(top, -1e30)
+    tot[...] = jnp.zeros_like(tot)
+    acc[...] = jnp.zeros_like(acc)
+    for one in loads:
+        one.wait()
+
+    def copy(i, src, h, way, peer):
+        b = bufs[i]
+        return remote(
+            b.at[src, h], b.at[src, h], send_sem.at[i, src, h, way], recv_sem.at[i, src, h],
+            (peer, t),
+        )
+
+    def source(k):
+        low = jnp.minimum(z, z_count - 1 - z)
+        both = k <= 2 * low
+        dist = jnp.where(both, (k + 1) // 2, k - low)
+        up = jnp.where(both, k % 2 == 1, z < z_count - 1 - z)
+        return jnp.where(up, z + dist, z - dist)
+
+    def reach(h, way, at):
+        return at <= z_count - 2 + h if way == 0 else at >= h
+
+    def flow(k, act_recv, act_send):
+        zz = source(k)
+        src = zz * x_count + x
+        for n in range(2):
+            for way, (ok, peer) in enumerate(targets):
+                side = zz <= z if way == 0 else zz >= z
+                h = 1 - n if way == 0 else n
+                came = (zz != z) & side & reach(h, way, z)
+                goes = ok & side & reach(h, way, z + 1 if way == 0 else z - 1)
+                for i in range(3):
+                    if act_recv:
+
+                        @pl.when(came)
+                        def _():
+                            copy(i, src, h, 0, s).wait_recv()
+
+                    @pl.when(goes)
+                    def _():
+                        act_send(copy(i, src, h, way, peer))
+
+                    @pl.when(side & (h == mine) & ((zz != z) | (way == 0)))
+                    def _():
+                        for j in range(1, x_count):
+                            act_send(
+                                copy(i, src, h, 1 + j, z * x_count + (x + j) % x_count)
+                            )
+
+    def update(i, queries, keys, values_t, bias):
+        sc = jnp.dot(keys, queries, preferred_element_type=F32) * factor
+        if bias != 0.0:
+            sc = sc + bias
+        old = top[i]
+        new = jnp.maximum(old, jnp.max(sc, axis=0, keepdims=True))
+        p = jnp.exp2(sc - new)
+        f = jnp.exp2(old - new)
+        top[i] = new
+        tot[i] = tot[i] * f + jnp.sum(p, axis=0, keepdims=True)
+        acc[i] = acc[i] * f + jnp.dot(values_t, p.astype(BF16), preferred_element_type=F32)
+
+    def block(src):
+        def tile(i, carry):
+            update(i, qb[i // group, i % group], kb[src, mine], vb[src, mine], 0.0)
+            return carry
+
+        lax.fori_loop(0, 2 * group, tile, 0)
+
+    def step(k, carry):
+        flow(k, True, lambda one: one.start())
+
+        @pl.when(k == 0)
+        def _():
+            swap_q.wait_recv()
+
+        block(source(k) * x_count + x)
+
+        @pl.when(k > 0)
+        def _():
+            before = source(k - 1)
+            for j in range(1, x_count):
+                old = before * x_count + (x + j) % x_count
+                for i in range(3):
+                    copy(i, old, mine, 0, s).wait_recv()
+                block(old)
+
+        return carry
+
+    lax.fori_loop(0, z_count, step, 0)
+    final = source(z_count - 1)
+    ends = [final * x_count + (x + j) % x_count for j in range(1, x_count)]
+    for src in ends:
+        copy(0, src, mine, 0, s).wait_recv()
+    keys = jnp.concatenate([cb[j, mine, 0] for j in range(sp_count)], axis=0)
+    vals = jnp.concatenate([cb[j, mine, 1] for j in range(sp_count)], axis=0)
+    vals = vals.astype(F32).T.astype(BF16)
+    for i in range(2 * group):
+        update(i, qb[i // group, i % group], keys, vals, lift * math.log2(math.e))
+    for src in ends:
+        for i in (1, 2):
+            copy(i, src, mine, 0, s).wait_recv()
+        block(src)
+    span = group * head_dim
+    for g in range(group):
+        ab[0, :, g * head_dim : (g + 1) * head_dim] = (acc[g] / tot[g]).T.astype(BF16)
+    swap_a = remote(ab.at[0], ab.at[1], swap_sem.at[2], swap_sem.at[3], (mate, t))
+    swap_a.start()
+    for g in range(group):
+        at = pl.ds(pl.multiple_of(mine * span + g * head_dim, head_dim), head_dim)
+        out_ref[:, at] = (acc[group + g] / tot[group + g]).T.astype(BF16)
+
+    def drain(k, carry):
+        flow(k, False, lambda one: one.wait_send())
+        return carry
+
+    lax.fori_loop(0, z_count, drain, 0)
+    swap_a.wait_recv()
+    out_ref[:, pl.ds(pl.multiple_of((1 - mine) * span, head_dim), span)] = ab[1]
+    swap_q.wait_send()
+    swap_a.wait_send()
 
 
 def mix_kernel(
@@ -437,18 +604,17 @@
         [cond[None], ctx_cond[None], jnp.zeros((6, cond.shape[0]), F32)], axis=0
     )
     sds = jax.ShapeDtypeStruct
-    qt, k, vt, ck, cv, gate = pl.pallas_call(
+    qt, k, vt, ckv, gate = pl.pallas_call(
         functools.partial(front_kernel, sp_count, tp_count, head_dim),
         out_shape=[
             sds((heads, head_dim, all_rows), BF16),
             sds((kv_heads, all_rows, head_dim), BF16),
             sds((kv_heads, head_dim, all_rows), BF16),
-            sds((kv_heads, ctx_rows, head_dim), BF16),
-            sds((kv_heads, ctx_rows, head_dim), BF16),
+            sds((kv_heads, 2, ctx_rows, head_dim), BF16),
             sds((1, width), F32),
         ],
         in_specs=[VM, ANY, ANY, VM, ANY, ANY, ANY, VM, VM, VM, VM],
-        out_specs=[VM] * 6,
+        out_specs=[VM] * 5,
         scratch_shapes=[
             pltpu.VMEM(mod_weight.shape, F32),
             pltpu.VMEM((tp_count, rows, width), BF16),
@@ -468,7 +634,7 @@
             DMA((tp_count,)),
         ],
         compiler_params=pltpu.CompilerParams(
-            collective_id=0, has_side_effects=True, vmem_limit_bytes=48 << 20
+            collective_id=0, has_side_effects=True, vmem_limit_bytes=VMEM_BYTES
         ),
         name="front",
     )(
@@ -477,27 +643,40 @@
     )
 
     lift = math.log(sp_count * all_rows / (2.0 * sp_count * ctx_rows))
+    group = heads // kv_heads
+    paired = kv_heads == 2 and (sp_count // x_count) % 2 == 0
+    scratch = [
+        pltpu.VMEM((sp_count, kv_heads, all_rows, head_dim), BF16),
+        pltpu.VMEM((sp_count, kv_heads, head_dim, all_rows), BF16),
+        pltpu.VMEM((sp_count, kv_heads, 2, ctx_rows, head_dim), BF16),
+        pltpu.VMEM((heads, 1, all_rows), F32),
+        pltpu.VMEM((heads, 1, all_rows), F32),
+        pltpu.VMEM((heads, head_dim, all_rows), F32),
+        DMA((3,)),
+    ]
+    if paired:
+        scratch += [
+            pltpu.VMEM((2, group, head_dim, all_rows), BF16),
+            pltpu.VMEM((2, all_rows, group * head_dim), BF16),
+            DMA((3, sp_count, 2, x_count + 1)),
+            DMA((3, sp_count, 2)),
+            DMA((4,)),
+        ]
+    else:
+        scratch += [DMA((3, sp_count, x_count + 1)), DMA((3, sp_count))]
     att = pl.pallas_call(
-        functools.partial(attend_kernel, sp_count, x_count, heads // kv_heads, lift),
+        functools.partial(
+            pair_kernel if paired else attend_kernel, sp_count, x_count, group, lift
+        ),
         out_shape=sds((all_rows, heads * head_dim), BF16),
-        in_specs=[ANY, ANY, ANY, ANY, VM],
+        in_specs=[ANY, ANY, ANY, VM],
         out_specs=VM,
-        scratch_shapes=[
-            pltpu.VMEM((sp_count, kv_heads, all_rows, head_dim), BF16),
-            pltpu.VMEM((sp_count, kv_heads, head_dim, all_rows), BF16),
-            pltpu.VMEM((sp_count, 2, kv_heads, ctx_rows, head_dim), BF16),
-            pltpu.VMEM((heads, 1, all_rows), F32),
-            pltpu.VMEM((heads, 1, all_rows), F32),
-            pltpu.VMEM((heads, head_dim, all_rows), F32),
-            DMA((4,)),
-            DMA((3, sp_count, x_count + 1)),
-            DMA((3, sp_count)),
-        ],
+        scratch_shapes=scratch,
         compiler_params=pltpu.CompilerParams(
-            collective_id=1, has_side_effects=True, vmem_limit_bytes=48 << 20
+            collective_id=1, has_side_effects=True, vmem_limit_bytes=VMEM_BYTES
         ),
         name="attend",
-    )(k, vt, ck, cv, qt)
+    )(k, vt, ckv, qt)
 
     chunks = 4
     y_count = tp_count // 2
@@ -520,7 +699,7 @@
             DMA((chunks, far)),
         ],
         compiler_params=pltpu.CompilerParams(
-            collective_id=2, has_side_effects=True, vmem_limit_bytes=48 << 20
+            collective_id=2, has_side_effects=True, vmem_limit_bytes=VMEM_BYTES
         ),
         name="mix",
     )(att, out_weight, latents, gate)

time: 114 us -> 111 us (0.974)
  the two profiles are of different devices: /device:TPU:0 before, /device:TPU:17 now
where the time goes in v2:
time: 111 us
  Pallas kernels  105 us (95%)
  other arithmetic  3.36 us (3%)
  local copies, waits for them, and re-layouts  1.96 us (2%)
    pallas_call x1, Pallas kernels, body(): pl.pallas_call(functools.partial(pair_kernel if paired else attend_kernel...  60.1 us
    pallas_call x1, Pallas kernels, body(): pl.pallas_call(functools.partial(front_kernel, sp_count, tp_count, head_d...  25 us
    pallas_call x1, Pallas kernels, body(): pl.pallas_call(functools.partial(mix_kernel, tp_count, chunks), out_shape...  20.5 us

profile of v2, /device:TPU:17, one launch (start us, length us, event | category | flops | bytes accessed | tf_op | source)
XLA Modules:
  0.0 110.9 jit_solution(15543254467576505171)
XLA Ops:
  0.0 0.1 pad.10.clone
  0.1 1.4 %maximum_maximum_fusion.cond_ref = f32[8,256]{1,0:T(8,128)} fusion(f32[1,256]{1,0:T(1,128)} %bitcast.4, f32[1,256]{1,0:T(1,128)} %bitcast.5, f32[8]{0:T(128)S(1)} %pad.10.clone), kind=kLoop, calls=%fused_computation.8 | loop fusion | flops 4096 | bytes 10272 | tf_op jit(solution)/shard_map/concatenate | solution.py:603
  1.5 0.5 fusion
  2.0 0.7 pad_maximum_fusion.1.sin_ref
  2.7 0.7 pad_maximum_fusion.cos_ref
  3.5 25.0 %front.1 = (bf16[4,128,512]{2,1,0:T(8,128)(2,1)}, bf16[2,512,128]{2,1,0:T(8,128)(2,1)}, bf16[2,128,512]{2,1,0:T(8,128)(2,1)}, bf16[2,2,64,128]{3,2,1,0:T(8,128)(2,1)}, f32[1,2048]{1,0:T(1,128)}) custom-call(f32[8,256]{1,0:T(8,128)} %maximum_maximum_fusion.cond_ref, f32[256,1536]{1,0:T(8,128)} %mw_hbm.1, bf16[128,2048]{1,0:T(8,128)(2,1)} %lat_ref.1, ...), custom_call_target="tpu_custom_call" | custom-call | tf_op jit(solution)/shard_map/front/pallas_call | solution.py:607
  28.4 60.1 %attend.1.att_ref = bf16[512,512]{1,0:T(8,128)(2,1)} custom-call(bf16[2,512,128]{2,1,0:T(8,128)(2,1)} %get-tuple-element.10.k_hbm, bf16[2,128,512]{2,1,0:T(8,128)(2,1)} %get-tuple-element.11.vt_hbm, bf16[2,2,64,128]{3,2,1,0:T(8,128)(2,1)} %get-tuple-element.12.ckv_hbm, bf16[4,128,512]{2,1,0:T(8,128)(2,1)} %get-tuple-element.13.qt_ref), custom_call_target="tpu_custom_call" | custom-call | tf_op jit(solution)/shard_map/attend/pallas_call | solution.py:667
  88.5 20.5 %mix.1 = bf16[128,2048]{1,0:T(8,128)(2,1)} custom-call(bf16[512,512]{1,0:T(8,128)(2,1)} %attend.1.att_ref, bf16[512,2048]{1,0:T(8,128)(2,1)} %wo_ref.1, bf16[128,2048]{1,0:T(8,128)(2,1)} %lat_ref.1, f32[1,2048]{1,0:T(1,128)} %get-tuple-element.14.gate_ref), custom_call_target="tpu_custom_call" | custom-call | tf_op jit(solution)/shard_map/mix/pallas_call | solution.py:685
  109.0 1.9 %copy.13 = bf16[128,2048]{1,0:T(8,128)(2,1)} copy(bf16[128,2048]{1,0:T(8,128)(2,1)} %mix.1) | data formatting | bytes 1048576
  (3 shorter events, 0.0 us)

commit v3 on v2

--- a/solution.py
+++ b/solution.py
@@ -27,12 +27,9 @@
 def tables(positions, head_dim):
     quarter = head_dim // 4
     inv_freq = ROPE_BASE ** (-jnp.arange(quarter, dtype=F32) / quarter)
-    row_ang = inv_freq[:, None] * (positions // GRID_W).astype(F32)[None, :]
-    col_ang = inv_freq[:, None] * (positions % GRID_W).astype(F32)[None, :]
-    cos = jnp.concatenate([jnp.cos(row_ang)] * 2 + [jnp.cos(col_ang)] * 2, axis=0)
-    row_sin, col_sin = jnp.sin(row_ang), jnp.sin(col_ang)
-    sin = jnp.concatenate([-row_sin, row_sin, -col_sin, col_sin], axis=0)
-    return cos, sin
+    where = jnp.stack([positions // GRID_W, positions % GRID_W]).astype(F32)
+    angles = where[:, None, :] * inv_freq[None, :, None]
+    return jnp.cos(angles), jnp.sin(angles)
 
 
 def remote(src, dst, send, recv, dev):
@@ -136,10 +133,12 @@
     qgain, kgain = qg_ref[...], kg_ref[...]
 
     def turn(yt, cos, sin):
-        part_t = jnp.concatenate(
-            [yt[q4 : 2 * q4], yt[:q4], yt[3 * q4 :], yt[2 * q4 : 3 * q4]], axis=0
-        )
-        return yt * cos + part_t * sin
+        out = []
+        for n in range(2):
+            a = yt[2 * n * q4 : (2 * n + 1) * q4]
+            b = yt[(2 * n + 1) * q4 : (2 * n + 2) * q4]
+            out += [a * cos[n] - b * sin[n], b * cos[n] + a * sin[n]]
+        return jnp.concatenate(out, axis=0)
 
     def unit(yh, gain):
         return yh * lax.rsqrt(jnp.mean(yh * yh, axis=-1, keepdims=True) + NORM_EPS) * gain
@@ -162,7 +161,7 @@
             xn[i * rows : (i + 1) * rows, :] = modulate(lat[yy * 2 + i], 0)
         x = xn[...]
         at = pl.ds(pl.multiple_of(yy * span, span), span)
-        cos, sin = cos_ref[:, at], sin_ref[:, at]
+        cos, sin = cos_ref[:, :, at], sin_ref[:, :, at]
         for w, kind in ((wq, 0), (wk, 1), (wv, 2)):
             step = min(2 * head_dim, w.shape[1])
             for n in range(0, w.shape[1], step):
@@ -357,21 +356,13 @@
     for one in loads:
         one.start()
     barrier = pltpu.get_barrier_semaphore()
-    targets = []
-    for sign in (1, -1):
-        ok = (z + sign >= 0) & (z + sign < z_count)
-        peer = ((z + sign + z_count) % z_count) * x_count + x
-        targets.append((ok, peer))
-
-        @pl.when(ok)
-        def _():
-            pl.semaphore_signal(barrier, inc=1, device_id=(peer, t), device_id_type=MESH)
-
+    for j in range(1, z_count):
+        peer = (z + j) % z_count * x_count + x
+        pl.semaphore_signal(barrier, inc=1, device_id=(peer, t), device_id_type=MESH)
     for j in range(1, x_count):
         peer = z * x_count + (x + j) % x_count
         pl.semaphore_signal(barrier, inc=1, device_id=(peer, t), device_id_type=MESH)
-    ends_here = (z == 0).astype(jnp.int32) + (z == z_count - 1).astype(jnp.int32)
-    pl.semaphore_wait(barrier, x_count + 1 - ends_here)
+    pl.semaphore_wait(barrier, x_count + z_count - 2)
 
     swap_q = remote(
         qt_ref.at[pl.ds((1 - mine) * group, group)], qb.at[0],
@@ -388,8 +379,7 @@
     def copy(i, src, h, way, peer):
         b = bufs[i]
         return remote(
-            b.at[src, h], b.at[src, h], send_sem.at[i, src, h, way], recv_sem.at[i, src, h],
-            (peer, t),
+            b.at[src, h], b.at[src, h], send_sem.at[i, way], recv_sem.at[i, src], (peer, t)
         )
 
     def source(k):
@@ -399,35 +389,31 @@
         up = jnp.where(both, k % 2 == 1, z < z_count - 1 - z)
         return jnp.where(up, z + dist, z - dist)
 
-    def reach(h, way, at):
-        return at <= z_count - 2 + h if way == 0 else at >= h
-
-    def flow(k, act_recv, act_send):
+    def line(act):
+        for dist in range(1, z_count):
+            for sign in (1, -1):
+                there = z + sign * dist
+
+                @pl.when((there >= 0) & (there < z_count))
+                def _():
+                    to = (there + z_count) % z_count
+                    for i in range(3):
+                        act(copy(i, s, to % 2, to, to * x_count + x))
+
+    def across(k, act):
         zz = source(k)
         src = zz * x_count + x
-        for n in range(2):
-            for way, (ok, peer) in enumerate(targets):
-                side = zz <= z if way == 0 else zz >= z
-                h = 1 - n if way == 0 else n
-                came = (zz != z) & side & reach(h, way, z)
-                goes = ok & side & reach(h, way, z + 1 if way == 0 else z - 1)
-                for i in range(3):
-                    if act_recv:
-
-                        @pl.when(came)
-                        def _():
-                            copy(i, src, h, 0, s).wait_recv()
-
-                    @pl.when(goes)
-                    def _():
-                        act_send(copy(i, src, h, way, peer))
-
-                    @pl.when(side & (h == mine) & ((zz != z) | (way == 0)))
-                    def _():
-                        for j in range(1, x_count):
-                            act_send(
-                                copy(i, src, h, 1 + j, z * x_count + (x + j) % x_count)
-                            )
+        for i in range(3):
+            if act is None:
+
+                @pl.when(k > 0)
+                def _():
+                    copy(i, src, mine, 0, s).wait_recv()
+
+            for j in range(1, x_count):
+                way = z_count + zz * (x_count - 1) + j - 1
+                one = copy(i, src, mine, way, z * x_count + (x + j) % x_count)
+                one.start() if act is None else act(one)
 
     def update(i, queries, keys, values_t, bias):
         sc = jnp.dot(keys, queries, preferred_element_type=F32) * factor
@@ -449,7 +435,7 @@
         lax.fori_loop(0, 2 * group, tile, 0)
 
     def step(k, carry):
-        flow(k, True, lambda one: one.start())
+        across(k, None)
 
         @pl.when(k == 0)
         def _():
@@ -468,6 +454,7 @@
 
         return carry
 
+    line(lambda one: one.start())
     lax.fori_loop(0, z_count, step, 0)
     final = source(z_count - 1)
     ends = [final * x_count + (x + j) % x_count for j in range(1, x_count)]
@@ -476,26 +463,34 @@
     keys = jnp.concatenate([cb[j, mine, 0] for j in range(sp_count)], axis=0)
     vals = jnp.concatenate([cb[j, mine, 1] for j in range(sp_count)], axis=0)
     vals = vals.astype(F32).T.astype(BF16)
-    for i in range(2 * group):
-        update(i, qb[i // group, i % group], keys, vals, lift * math.log2(math.e))
-    for src in ends:
-        for i in (1, 2):
-            copy(i, src, mine, 0, s).wait_recv()
-        block(src)
     span = group * head_dim
-    for g in range(group):
-        ab[0, :, g * head_dim : (g + 1) * head_dim] = (acc[g] / tot[g]).T.astype(BF16)
     swap_a = remote(ab.at[0], ab.at[1], swap_sem.at[2], swap_sem.at[3], (mate, t))
-    swap_a.start()
-    for g in range(group):
-        at = pl.ds(pl.multiple_of(mine * span + g * head_dim, head_dim), head_dim)
-        out_ref[:, at] = (acc[group + g] / tot[group + g]).T.astype(BF16)
+    for who in range(2):
+        for g in range(group):
+            update(who * group + g, qb[who, g], keys, vals, lift * math.log2(math.e))
+        for src in ends:
+            if who == 0:
+                for i in (1, 2):
+                    copy(i, src, mine, 0, s).wait_recv()
+            for g in range(group):
+                update(who * group + g, qb[who, g], kb[src, mine], vb[src, mine], 0.0)
+        for g in range(group):
+            i = who * group + g
+            done = (acc[i] / tot[i]).T.astype(BF16)
+            if who == 0:
+                ab[0, :, g * head_dim : (g + 1) * head_dim] = done
+            else:
+                at = pl.ds(pl.multiple_of(mine * span + g * head_dim, head_dim), head_dim)
+                out_ref[:, at] = done
+        if who == 0:
+            swap_a.start()
 
     def drain(k, carry):
-        flow(k, False, lambda one: one.wait_send())
+        across(k, lambda one: one.wait_send())
         return carry
 
     lax.fori_loop(0, z_count, drain, 0)
+    line(lambda one: one.wait_send())
     swap_a.wait_recv()
     out_ref[:, pl.ds(pl.multiple_of((1 - mine) * span, head_dim), span)] = ab[1]
     swap_q.wait_send()
@@ -658,8 +653,8 @@
         scratch += [
             pltpu.VMEM((2, group, head_dim, all_rows), BF16),
             pltpu.VMEM((2, all_rows, group * head_dim), BF16),
-            DMA((3, sp_count, 2, x_count + 1)),
-            DMA((3, sp_count, 2)),
+            DMA((3, sp_count)),
+            DMA((3, sp_count)),
             DMA((4,)),
         ]
     else:
@@ -699,7 +694,7 @@
             DMA((chunks, far)),
         ],
         compiler_params=pltpu.CompilerParams(
-            collective_id=2, has_side_effects=True, vmem_limit_bytes=VMEM_BYTES
+            collective_id=2, has_side_effects=True, vmem_limit_bytes=40 << 20
         ),
         name="mix",
     )(att, out_weight, latents, gate)

time: 111 us -> 102 us (0.919)
  the two profiles are of different devices: /device:TPU:17 before, /device:TPU:0 now
where the time goes in v3:
time: 102 us; the launch traced here: 101 us
  Pallas kernels  93.6 us (92%)
  local copies, waits for them, and re-layouts  5.24 us (5%)
  other arithmetic  2.63 us (3%)
    pallas_call x1, Pallas kernels, body(): pl.pallas_call(functools.partial(pair_kernel if paired else attend_kernel...  49.1 us
    pallas_call x1, Pallas kernels, body(): pl.pallas_call(functools.partial(front_kernel, sp_count, tp_count, head_d...  27.8 us
    pallas_call x1, Pallas kernels, body(): pl.pallas_call(functools.partial(mix_kernel, tp_count, chunks), out_shape...  16.7 us
    unnamed x9, local copies, waits for them, and re-layouts  5.16 us

profile of v3, /device:TPU:0, one launch (start us, length us, event | category | flops | bytes accessed | tf_op | source)
XLA Modules:
  0.0 101.5 jit_solution(12938262403114184358)
XLA Ops:
  0.0 0.1 pad.4.clone
  0.1 1.4 %maximum_maximum_fusion.cond_ref = f32[8,256]{1,0:T(8,128)} fusion(f32[1,256]{1,0:T(1,128)} %bitcast.4, f32[1,256]{1,0:T(1,128)} %bitcast.5, f32[8]{0:T(128)S(1)} %pad.4.clone), kind=kLoop, calls=%fused_computation.2 | loop fusion | flops 4096 | bytes 10272 | tf_op jit(solution)/shard_map/concatenate | solution.py:598
  1.5 1.2 %multiply_sine_fusion = (f32[2,32,512]{2,1,0:T(8,128)}, f32[2,32,512]{2,1,0:T(8,128)}) fusion(f32[32]{0:T(128)S(1)} %multiply_power_fusion, f32[2,512]{1,0:T(2,128)S(1)} %add_convert_fusion), kind=kLoop, calls=%fused_computation | loop fusion | flops 32768 | bytes 266368 | tf_op jit(solution)/shard_map/sin | solution.py:32
  2.7 27.8 %front.1 = (bf16[4,128,512]{2,1,0:T(8,128)(2,1)}, bf16[2,512,128]{2,1,0:T(8,128)(2,1)}, bf16[2,128,512]{2,1,0:T(8,128)(2,1)}, bf16[2,2,64,128]{3,2,1,0:T(8,128)(2,1)}, f32[1,2048]{1,0:T(1,128)}) custom-call(f32[8,256]{1,0:T(8,128)} %maximum_maximum_fusion.cond_ref, f32[256,1536]{1,0:T(8,128)} %mw_hbm.1, bf16[128,2048]{1,0:T(8,128)(2,1)} %lat_ref.1, ...), custom_call_target="tpu_custom_call" | custom-call | tf_op jit(solution)/shard_map/front/pallas_call | solution.py:602
  30.5 49.1 %attend.1.att_ref = bf16[512,512]{1,0:T(8,128)(2,1)} custom-call(bf16[2,512,128]{2,1,0:T(8,128)(2,1)} %get-tuple-element.10.k_hbm, bf16[2,128,512]{2,1,0:T(8,128)(2,1)} %get-tuple-element.11.vt_hbm, bf16[2,2,64,128]{3,2,1,0:T(8,128)(2,1)} %get-tuple-element.12.ckv_hbm, bf16[4,128,512]{2,1,0:T(8,128)(2,1)} %get-tuple-element.13.qt_ref), custom_call_target="tpu_custom_call" | custom-call | tf_op jit(solution)/shard_map/attend/pallas_call | solution.py:662
  79.6 0.0 copy-start
  79.6 1.0 %copy-done = bf16[128,2048]{1,0:T(8,128)(2,1)S(1)} copy-done((bf16[128,2048]{1,0:T(8,128)(2,1)S(1)}, bf16[128,2048]{1,0:T(8,128)(2,1)}, u32[]{:S(2)}) %copy-start) | copy-done | bytes 524312
  80.6 0.0 copy-start.1
  80.6 1.0 %copy-done.1 = bf16[512,512]{1,0:T(8,128)(2,1)S(1)} copy-done((bf16[512,512]{1,0:T(8,128)(2,1)S(1)}, bf16[512,512]{1,0:T(8,128)(2,1)}, u32[]{:S(2)}) %copy-start.1) | copy-done | bytes 524312
  81.7 0.0 copy-start.2
  81.7 1.6 %copy-done.2 = bf16[512,2048]{1,0:T(8,128)(2,1)S(1)} copy-done((bf16[512,2048]{1,0:T(8,128)(2,1)S(1)}, bf16[512,2048]{1,0:T(8,128)(2,1)}, u32[]{:S(2)}) %copy-start.2) | copy-done | bytes 2097176
  83.3 0.0 copy-start.3
  83.3 0.7 copy-done.3
  84.0 16.7 %mix.1 = bf16[128,2048]{1,0:T(8,128)(2,1)S(1)} custom-call(bf16[512,512]{1,0:T(8,128)(2,1)S(1)} %copy-done.1, bf16[512,2048]{1,0:T(8,128)(2,1)S(1)} %copy-done.2, bf16[128,2048]{1,0:T(8,128)(2,1)S(1)} %copy-done, f32[1,2048]{1,0:T(1,128)S(1)} %copy-done.3), custom_call_target="tpu_custom_call" | custom-call | tf_op jit(solution)/shard_map/mix/pallas_call | solution.py:680
  100.7 0.8 copy.13
  (4 shorter events, 0.0 us)
Async XLA Ops:
  79.6 1.0 %copy-start = (bf16[128,2048]{1,0:T(8,128)(2,1)S(1)}, bf16[128,2048]{1,0:T(8,128)(2,1)}, u32[]{:S(2)}) copy-start(bf16[128,2048]{1,0:T(8,128)(2,1)} %lat_ref.1) | copy-start | bytes 1572868
  80.6 1.0 %copy-start.1 = (bf16[512,512]{1,0:T(8,128)(2,1)S(1)}, bf16[512,512]{1,0:T(8,128)(2,1)}, u32[]{:S(2)}) copy-start(bf16[512,512]{1,0:T(8,128)(2,1)} %attend.1.att_ref) | copy-start | bytes 1572868
  81.7 1.6 %copy-start.2 = (bf16[512,2048]{1,0:T(8,128)(2,1)S(1)}, bf16[512,2048]{1,0:T(8,128)(2,1)}, u32[]{:S(2)}) copy-start(bf16[512,2048]{1,0:T(8,128)(2,1)} %wo_ref.1) | copy-start | bytes 6291460
  83.3 0.7 copy-start.3

commit v4 on v3

--- a/solution.py
+++ b/solution.py
@@ -44,6 +44,7 @@
     qt_ref, k_ref, vt_ref, ckv_ref, gate_ref,
     mw, lat, wq, wk, wv, part, tot, mod, xn, load_sem,
     lat_send, lat_recv, part_send, part_recv, tot_send, tot_recv,
+    wo_hbm, wo_vm, wo_sem,
 ):
     s, t = lax.axis_index("sp"), lax.axis_index("tp")
     y, c = t // 2, t % 2
@@ -61,6 +62,8 @@
     ]
     for one in loads:
         one.start()
+
+    pltpu.make_async_copy(wo_hbm, wo_vm, wo_sem.at[0]).start()
 
     barrier = pltpu.get_barrier_semaphore()
     for j in range(1, sp_count):
@@ -204,23 +207,11 @@
     ]
     for one in loads:
         one.start()
-    barrier = pltpu.get_barrier_semaphore()
     targets = []
     for sign in (1, -1):
         ok = (z + sign >= 0) & (z + sign < z_count)
         peer = ((z + sign + z_count) % z_count) * x_count + x
         targets.append((ok, peer))
-    for ok, peer in targets:
-
-        @pl.when(ok)
-        def _():
-            pl.semaphore_signal(barrier, inc=1, device_id=(peer, t), device_id_type=MESH)
-
-    for j in range(1, x_count):
-        peer = z * x_count + (x + j) % x_count
-        pl.semaphore_signal(barrier, inc=1, device_id=(peer, t), device_id_type=MESH)
-    ends_here = (z == 0).astype(jnp.int32) + (z == z_count - 1).astype(jnp.int32)
-    pl.semaphore_wait(barrier, x_count + 1 - ends_here)
 
     top[...] = jnp.full_like(top, -1e30)
     tot[...] = jnp.zeros_like(tot)
@@ -355,15 +346,6 @@
     ]
     for one in loads:
         one.start()
-    barrier = pltpu.get_barrier_semaphore()
-    for j in range(1, z_count):
-        peer = (z + j) % z_count * x_count + x
-        pl.semaphore_signal(barrier, inc=1, device_id=(peer, t), device_id_type=MESH)
-    for j in range(1, x_count):
-        peer = z * x_count + (x + j) % x_count
-        pl.semaphore_signal(barrier, inc=1, device_id=(peer, t), device_id_type=MESH)
-    pl.semaphore_wait(barrier, x_count + z_count - 2)
-
     swap_q = remote(
         qt_ref.at[pl.ds((1 - mine) * group, group)], qb.at[0],
         swap_sem.at[0], swap_sem.at[1], (mate, t),
@@ -499,7 +481,7 @@
 
 def mix_kernel(
     tp_count, chunks,
-    att_ref, wo_ref, lat_ref, gate_ref,
+    att_ref, wo_hbm, wo_ref, wo_sem, lat_ref, gate_ref,
     out_ref,
     core_out, core_in, mesh_out, mesh_in, mixed, core_send, core_recv, mesh_send, mesh_recv,
 ):
@@ -509,11 +491,8 @@
     partner = y * 2 + 1 - c
     rows, width = lat_ref.shape
     step = width // chunks
-    barrier = pltpu.get_barrier_semaphore()
     peers = [((y + j) % y_count) * 2 + c for j in range(1, y_count)]
-    for peer in peers + [partner]:
-        pl.semaphore_signal(barrier, inc=1, device_id=(s, peer), device_id_type=MESH)
-    pl.semaphore_wait(barrier, y_count)
+    pltpu.make_async_copy(wo_hbm, wo_ref, wo_sem.at[0]).wait()
 
     def piece(n, j, cc):
         yy = (y + j) % y_count
@@ -566,6 +545,24 @@
         one.wait_send()
 
 
+def whole_kernel(sp_count, tp_count, x_count, head_dim, group, lift, chunks, paired, counts, *refs):
+    (
+        cond, mw, lat, ctx, wq, wk, wv, qg, kg, cos, sin, wo, lat_rows,
+        out, qt, k, vt, ckv, gate, att, wo_vm, wo_sem, *rest,
+    ) = refs
+    front, middle, last = counts
+    front_scratch, middle_scratch = rest[:front], rest[front : front + middle]
+    front_kernel(
+        sp_count, tp_count, head_dim, cond, mw, lat, ctx, wq, wk, wv, qg, kg, cos, sin,
+        qt, k, vt, ckv, gate, *front_scratch, wo, wo_vm, wo_sem,
+    )
+    attention = pair_kernel if paired else attend_kernel
+    attention(sp_count, x_count, group, lift, k, vt, ckv, qt, att, *middle_scratch)
+    mix_kernel(
+        tp_count, chunks, att, wo, wo_vm, wo_sem, lat_rows, gate, out, *rest[front + middle :]
+    )
+
+
 ANY = pl.BlockSpec(memory_space=pl.ANY)
 VM = pl.BlockSpec(memory_space=pltpu.VMEM)
 DMA = pltpu.SemaphoreType.DMA
@@ -599,48 +596,42 @@
         [cond[None], ctx_cond[None], jnp.zeros((6, cond.shape[0]), F32)], axis=0
     )
     sds = jax.ShapeDtypeStruct
-    qt, k, vt, ckv, gate = pl.pallas_call(
-        functools.partial(front_kernel, sp_count, tp_count, head_dim),
-        out_shape=[
-            sds((heads, head_dim, all_rows), BF16),
-            sds((kv_heads, all_rows, head_dim), BF16),
-            sds((kv_heads, head_dim, all_rows), BF16),
-            sds((kv_heads, 2, ctx_rows, head_dim), BF16),
-            sds((1, width), F32),
-        ],
-        in_specs=[VM, ANY, ANY, VM, ANY, ANY, ANY, VM, VM, VM, VM],
-        out_specs=[VM] * 5,
-        scratch_shapes=[
-            pltpu.VMEM(mod_weight.shape, F32),
-            pltpu.VMEM((tp_count, rows, width), BF16),
-            pltpu.VMEM(query_weight.shape, BF16),
-            pltpu.VMEM(key_matrix.shape, BF16),
-            pltpu.VMEM(value_matrix.shape, BF16),
-            pltpu.VMEM((sp_count, 2, mod_cols), F32),
-            pltpu.VMEM((tp_count, 2, mod_cols), F32),
-            pltpu.VMEM((2, mod_cols * tp_count), F32),
-            pltpu.VMEM((2 * rows, width), BF16),
-            DMA((5,)),
-            DMA((tp_count,)),
-            DMA((tp_count,)),
-            DMA((sp_count,)),
-            DMA((sp_count,)),
-            DMA((tp_count,)),
-            DMA((tp_count,)),
-        ],
-        compiler_params=pltpu.CompilerParams(
-            collective_id=0, has_side_effects=True, vmem_limit_bytes=VMEM_BYTES
-        ),
-        name="front",
-    )(
-        pair, mod_weight, latents, context, query_weight, key_matrix, value_matrix,
-        query_gain[None], key_gain[None], cos, sin,
-    )
-
     lift = math.log(sp_count * all_rows / (2.0 * sp_count * ctx_rows))
     group = heads // kv_heads
     paired = kv_heads == 2 and (sp_count // x_count) % 2 == 0
-    scratch = [
+    chunks = 4
+    y_count = tp_count // 2
+    step = width // chunks
+    far = max(y_count - 1, 1)
+    shared = [
+        pltpu.VMEM((heads, head_dim, all_rows), BF16),
+        pltpu.VMEM((kv_heads, all_rows, head_dim), BF16),
+        pltpu.VMEM((kv_heads, head_dim, all_rows), BF16),
+        pltpu.VMEM((kv_heads, 2, ctx_rows, head_dim), BF16),
+        pltpu.VMEM((1, width), F32),
+        pltpu.VMEM((all_rows, heads * head_dim), BF16),
+        pltpu.VMEM(out_weight.shape, BF16),
+        DMA((1,)),
+    ]
+    front = [
+        pltpu.VMEM(mod_weight.shape, F32),
+        pltpu.VMEM((tp_count, rows, width), BF16),
+        pltpu.VMEM(query_weight.shape, BF16),
+        pltpu.VMEM(key_matrix.shape, BF16),
+        pltpu.VMEM(value_matrix.shape, BF16),
+        pltpu.VMEM((sp_count, 2, mod_cols), F32),
+        pltpu.VMEM((tp_count, 2, mod_cols), F32),
+        pltpu.VMEM((2, mod_cols * tp_count), F32),
+        pltpu.VMEM((2 * rows, width), BF16),
+        DMA((5,)),
+        DMA((tp_count,)),
+        DMA((tp_count,)),
+        DMA((sp_count,)),
+        DMA((sp_count,)),
+        DMA((tp_count,)),
+        DMA((tp_count,)),
+    ]
+    middle = [
         pltpu.VMEM((sp_count, kv_heads, all_rows, head_dim), BF16),
         pltpu.VMEM((sp_count, kv_heads, head_dim, all_rows), BF16),
         pltpu.VMEM((sp_count, kv_heads, 2, ctx_rows, head_dim), BF16),
@@ -650,7 +641,7 @@
         DMA((3,)),
     ]
     if paired:
-        scratch += [
+        middle += [
             pltpu.VMEM((2, group, head_dim, all_rows), BF16),
             pltpu.VMEM((2, all_rows, group * head_dim), BF16),
             DMA((3, sp_count)),
@@ -658,46 +649,35 @@
             DMA((4,)),
         ]
     else:
-        scratch += [DMA((3, sp_count, x_count + 1)), DMA((3, sp_count))]
-    att = pl.pallas_call(
+        middle += [DMA((3, sp_count, x_count + 1)), DMA((3, sp_count))]
+    last = [
+        pltpu.VMEM((chunks, y_count, rows, step), BF16),
+        pltpu.VMEM((chunks, y_count, rows, step), BF16),
+        pltpu.VMEM((chunks, far, rows, step), BF16),
+        pltpu.VMEM((chunks, far, rows, step), BF16),
+        pltpu.VMEM((chunks, rows, step), F32),
+        DMA((chunks,)),
+        DMA((chunks,)),
+        DMA((chunks, far)),
+        DMA((chunks, far)),
+    ]
+    counts = (len(front), len(middle), len(last))
+    return pl.pallas_call(
         functools.partial(
-            pair_kernel if paired else attend_kernel, sp_count, x_count, group, lift
+            whole_kernel, sp_count, tp_count, x_count, head_dim, group, lift, chunks, paired, counts
         ),
-        out_shape=sds((all_rows, heads * head_dim), BF16),
-        in_specs=[ANY, ANY, ANY, VM],
+        out_shape=jax.ShapeDtypeStruct((rows, width), BF16),
+        in_specs=[VM, ANY, ANY, VM, ANY, ANY, ANY, VM, VM, VM, VM, ANY, VM],
         out_specs=VM,
-        scratch_shapes=scratch,
+        scratch_shapes=shared + front + middle + last,
         compiler_params=pltpu.CompilerParams(
-            collective_id=1, has_side_effects=True, vmem_limit_bytes=VMEM_BYTES
+            collective_id=0, has_side_effects=True, vmem_limit_bytes=VMEM_BYTES
         ),
-        name="attend",
-    )(k, vt, ckv, qt)
-
-    chunks = 4
-    y_count = tp_count // 2
-    step = width // chunks
-    far = max(y_count - 1, 1)
-    return pl.pallas_call(
-        functools.partial(mix_kernel, tp_count, chunks),
-        out_shape=sds((rows, width), BF16),
-        in_specs=[VM] * 4,
-        out_specs=VM,
-        scratch_shapes=[
-            pltpu.VMEM((chunks, y_count, rows, step), BF16),
-            pltpu.VMEM((chunks, y_count, rows, step), BF16),
-            pltpu.VMEM((chunks, far, rows, step), BF16),
-            pltpu.VMEM((chunks, far, rows, step), BF16),
-            pltpu.VMEM((chunks, rows, step), F32),
-            DMA((chunks,)),
-            DMA((chunks,)),
-            DMA((chunks, far)),
-            DMA((chunks, far)),
-        ],
-        compiler_params=pltpu.CompilerParams(
-            collective_id=2, has_side_effects=True, vmem_limit_bytes=40 << 20
-        ),
-        name="mix",
-    )(att, out_weight, latents, gate)
+        name="whole",
+    )(
+        pair, mod_weight, latents, context, query_weight, key_matrix, value_matrix,
+        query_gain[None], key_gain[None], cos, sin, out_weight, latents,
+    )
 
 
 def solution(mesh):

time: 102 us -> 94.9 us (0.930)
  Pallas kernels: 93.6 us -> 89.6 us
  local copies, waits for them, and re-layouts: 5.24 us -> 1.96 us
    pallas_call x3 -> x1, Pallas kernels: 93.6 us -> 89.6 us  [body(): pl.pallas_call(functools.partial(whole_kernel, sp_count, tp_count, x_coun...]
    unnamed x9 -> x1, local copies, waits for them, and re-layouts: 5.16 us -> 1.88 us
where the time goes in v4:
time: 94.9 us; the launch traced here: 94.2 us
  Pallas kernels  89.6 us (94%)
  other arithmetic  2.63 us (3%)
  local copies, waits for them, and re-layouts  1.96 us (2%)
    pallas_call x1, Pallas kernels, body(): pl.pallas_call(functools.partial(whole_kernel, sp_count, tp_count, x_coun...  89.6 us

profile of v4, /device:TPU:0, one launch (start us, length us, event | category | flops | bytes accessed | tf_op | source)
XLA Modules:
  0.0 94.2 jit_solution(10549934121144065272)
XLA Ops:
  0.0 0.1 pad.4.clone
  0.1 1.4 %maximum_maximum_fusion.refs_0_ = f32[8,256]{1,0:T(8,128)} fusion(f32[1,256]{1,0:T(1,128)} %bitcast.4, f32[1,256]{1,0:T(1,128)} %bitcast.5, f32[8]{0:T(128)S(1)} %pad.4.clone), kind=kLoop, calls=%fused_computation.2 | loop fusion | flops 4096 | bytes 10272 | tf_op jit(solution)/shard_map/concatenate | solution.py:595
  1.5 1.2 %multiply_sine_fusion = (f32[2,32,512]{2,1,0:T(8,128)}, f32[2,32,512]{2,1,0:T(8,128)}) fusion(f32[32]{0:T(128)S(1)} %multiply_power_fusion, f32[2,512]{1,0:T(2,128)S(1)} %add_convert_fusion), kind=kLoop, calls=%fused_computation | loop fusion | flops 32768 | bytes 266368 | tf_op jit(solution)/shard_map/sin | solution.py:32
  2.7 89.6 %whole.1 = bf16[128,2048]{1,0:T(8,128)(2,1)} custom-call(f32[8,256]{1,0:T(8,128)} %maximum_maximum_fusion.refs_0_, f32[256,1536]{1,0:T(8,128)} %refs_1_.1, bf16[128,2048]{1,0:T(8,128)(2,1)} %refs_12_.1, bf16[64,2048]{1,0:T(8,128)(2,1)} %refs_3_.1, bf16[2048,512]{1,0:T(8,128)(2,1)} %refs_4_.1, bf16[2048,256]{1,0:T(8,128)(2,1)} %refs_5_.1, ...), custom_call_target="tpu_custom_call" | custom-call | tf_op jit(solution)/shard_map/whole/pallas_call | solution.py:665
  92.3 1.9 %copy.13 = bf16[128,2048]{1,0:T(8,128)(2,1)} copy(bf16[128,2048]{1,0:T(8,128)(2,1)} %whole.1) | data formatting | bytes 1048576
  (4 shorter events, 0.0 us)

commit v5 on v4

--- a/solution.py
+++ b/solution.py
@@ -40,7 +40,7 @@
 
 def front_kernel(
     sp_count, tp_count, head_dim,
-    cond_ref, mw_hbm, lat_hbm, ctx_ref, wq_hbm, wk_hbm, wv_hbm, qg_ref, kg_ref, cos_ref, sin_ref,
+    cond_ref, cond_1_ref, mw_hbm, lat_hbm, ctx_ref, wq_hbm, wk_hbm, wv_hbm, qg_ref, kg_ref, cos_ref, sin_ref,
     qt_ref, k_ref, vt_ref, ckv_ref, gate_ref,
     mw, lat, wq, wk, wv, part, tot, mod, xn, load_sem,
     lat_send, lat_recv, part_send, part_recv, tot_send, tot_recv,
@@ -82,7 +82,8 @@
         one.start()
 
     loads[0].wait()
-    cond = cond_ref[...]
+    lines = lax.broadcasted_iota(jnp.int32, (8, cond_ref.shape[1]), 0)
+    cond = jnp.where(lines == 0, cond_ref[...], jnp.where(lines == 1, cond_1_ref[...], 0.0))
     cond = cond * jax.nn.sigmoid(cond)
     part[s] = jnp.dot(
         cond, mw[...], precision=lax.Precision.HIGHEST, preferred_element_type=F32
@@ -507,22 +508,25 @@
         for n in range(chunks)
     ]
     sent = []
-    for n in range(chunks):
-        for j in order:
-            core_out[n, j] = piece(n, j, 1 - c).astype(BF16)
-        cores[n].start()
-    for n in range(chunks):
-        mine = [piece(n, j, c) for j in order]
-        cores[n].wait_recv()
-        for j, value in zip(order, mine):
-            value = value + core_in[n, j].astype(F32)
+    for n in range(chunks + 1):
+        if n < chunks:
+            for j in order:
+                core_out[n, j] = piece(n, j, 1 - c).astype(BF16)
+            cores[n].start()
+        if n == 0:
+            continue
+        m = n - 1
+        own = [piece(m, j, c) for j in order]
+        cores[m].wait_recv()
+        for j, value in zip(order, own):
+            value = value + core_in[m, j].astype(F32)
             if j == 0:
-                mixed[n] = value
+                mixed[m] = value
             else:
-                mesh_out[n, j - 1] = value.astype(BF16)
+                mesh_out[m, j - 1] = value.astype(BF16)
                 one = remote(
-                    mesh_out.at[n, j - 1], mesh_in.at[n, j - 1], mesh_send.at[n, j - 1],
-                    mesh_recv.at[n, j - 1], (s, peers[j - 1]),
+                    mesh_out.at[m, j - 1], mesh_in.at[m, j - 1], mesh_send.at[m, j - 1],
+                    mesh_recv.at[m, j - 1], (s, peers[j - 1]),
                 )
                 one.start()
                 sent.append(one)
@@ -547,13 +551,13 @@
 
 def whole_kernel(sp_count, tp_count, x_count, head_dim, group, lift, chunks, paired, counts, *refs):
     (
-        cond, mw, lat, ctx, wq, wk, wv, qg, kg, cos, sin, wo, lat_rows,
+        cond, cond_1, mw, lat, ctx, wq, wk, wv, qg, kg, cos, sin, wo, lat_rows,
         out, qt, k, vt, ckv, gate, att, wo_vm, wo_sem, *rest,
     ) = refs
     front, middle, last = counts
     front_scratch, middle_scratch = rest[:front], rest[front : front + middle]
     front_kernel(
-        sp_count, tp_count, head_dim, cond, mw, lat, ctx, wq, wk, wv, qg, kg, cos, sin,
+        sp_count, tp_count, head_dim, cond, cond_1, mw, lat, ctx, wq, wk, wv, qg, kg, cos, sin,
         qt, k, vt, ckv, gate, *front_scratch, wo, wo_vm, wo_sem,
     )
     attention = pair_kernel if paired else attend_kernel
@@ -592,10 +596,6 @@
     mod_cols = mod_weight.shape[1]
     positions = lax.axis_index("sp") * all_rows + jnp.arange(all_rows, dtype=jnp.int32)
     cos, sin = tables(positions, head_dim)
-    pair = jnp.concatenate(
-        [cond[None], ctx_cond[None], jnp.zeros((6, cond.shape[0]), F32)], axis=0
-    )
-    sds = jax.ShapeDtypeStruct
     lift = math.log(sp_count * all_rows / (2.0 * sp_count * ctx_rows))
     group = heads // kv_heads
     paired = kv_heads == 2 and (sp_count // x_count) % 2 == 0
@@ -667,7 +667,7 @@
             whole_kernel, sp_count, tp_count, x_count, head_dim, group, lift, chunks, paired, counts
         ),
         out_shape=jax.ShapeDtypeStruct((rows, width), BF16),
-        in_specs=[VM, ANY, ANY, VM, ANY, ANY, ANY, VM, VM, VM, VM, ANY, VM],
+        in_specs=[VM, VM, ANY, ANY, VM, ANY, ANY, ANY, VM, VM, VM, VM, ANY, VM],
         out_specs=VM,
         scratch_shapes=shared + front + middle + last,
         compiler_params=pltpu.CompilerParams(
@@ -675,7 +675,7 @@
         ),
         name="whole",
     )(
-        pair, mod_weight, latents, context, query_weight, key_matrix, value_matrix,
+        cond[None], ctx_cond[None], mod_weight, latents, context, query_weight, key_matrix, value_matrix,
         query_gain[None], key_gain[None], cos, sin, out_weight, latents,
     )
 

time: 94.9 us -> 92.9 us (0.979)
  other arithmetic: 2.63 us -> 1.28 us
    concatenate x1 -> x0, other arithmetic: 1.36 us -> none  [body(): jnp.concatenate([cond[None], ctx_cond[None], jnp.zeros((6, cond.shape[0])...]
where the time goes in v5:
time: 92.9 us; the launch traced here: 91.9 us
  Pallas kernels  88.7 us (95%)
  local copies, waits for them, and re-layouts  1.88 us (2%)
  other arithmetic  1.28 us (1%)
    pallas_call x1, Pallas kernels, body(): pl.pallas_call(functools.partial(whole_kernel, sp_count, tp_count, x_coun...  88.7 us
    unnamed x1, local copies, waits for them, and re-layouts  1.88 us

profile of v5, /device:TPU:0, one launch (start us, length us, event | category | flops | bytes accessed | tf_op | source)
XLA Modules:
  0.0 91.9 jit_solution(11282206700672822871)
XLA Ops:
  0.1 1.2 %multiply_sine_fusion = (f32[2,32,512]{2,1,0:T(8,128)}, f32[2,32,512]{2,1,0:T(8,128)}) fusion(f32[32]{0:T(128)S(1)} %multiply_power_fusion, f32[2,512]{1,0:T(2,128)S(1)} %add_convert_fusion), kind=kLoop, calls=%fused_computation | loop fusion | flops 32768 | bytes 266368 | tf_op jit(solution)/shard_map/sin | solution.py:32
  1.3 88.7 %whole.1 = bf16[128,2048]{1,0:T(8,128)(2,1)} custom-call(f32[1,256]{1,0:T(1,128)} %bitcast.4, f32[1,256]{1,0:T(1,128)} %bitcast.5, f32[256,1536]{1,0:T(8,128)} %refs_2_.1, bf16[128,2048]{1,0:T(8,128)(2,1)} %refs_13_.1, bf16[64,2048]{1,0:T(8,128)(2,1)} %refs_4_.1, bf16[2048,512]{1,0:T(8,128)(2,1)} %refs_5_.1, bf16[2048,256]{1,0:T(8,128)(2,1)} %refs_6_.1, ...), custom_call_target="tpu_custom_call" | custom-call | tf_op jit(solution)/shard_map/whole/pallas_call | solution.py:665
  90.0 1.9 %copy.13 = bf16[128,2048]{1,0:T(8,128)(2,1)} copy(bf16[128,2048]{1,0:T(8,128)(2,1)} %whole.1) | data formatting | bytes 1048576
  (3 shorter events, 0.0 us)
